TPU v7x, 32 devices: a whole 2x2x4 slice. The times are simulated.
32 devices in a mesh: kv: 8 (over z, y), tp: 4 (over x, core).
Axes of the slice: x: 2, y: 2, z: 4, core: 2. Of those that a mesh axis runs over, the one named last changes fastest.
Arguments:
- piece_tokens: bfloat16 [768, 4096], P('kv'), may hold values from -6 to 6
- step_tokens: bfloat16 [8, 4096], P('kv'), may hold values from -6 to 6
- in_gain: float32 [4096], replicated, may hold values from 0.1 to 1.9
- w_query: bfloat16 [4096, 8, 2, 128], P(None, 'tp'), may hold values from -0.09375 to 0.09375
- w_key: bfloat16 [4096, 8, 2, 128], P(None, 'tp'), may hold values from -0.15625 to 0.15625
- w_value: bfloat16 [4096, 8, 256], P(None, 'tp'), may hold values from -0.09375 to 0.09375
- w_out: bfloat16 [8, 256, 4096], P('tp'), may hold values from -0.125 to 0.125
- mix_ratio: float32 [8], P('tp'), may hold values from 0.3 to 0.8
- out_gain: float32 [256], replicated, may hold values from 0.1 to 1.9
- prompt_keys: bfloat16 [16384, 8, 2, 128], P('kv', 'tp'), may hold values from -630 to 630
- prompt_values: bfloat16 [16384, 8, 256], P('kv', 'tp'), may hold values from -6 to 6
- step_cache_keys: bfloat16 [8, 1024, 8, 2, 128], P(None, 'kv', 'tp'), may hold values from -630 to 630
- step_cache_values: bfloat16 [8, 1024, 8, 256], P(None, 'kv', 'tp'), may hold values from -6 to 6
- prompt_len: int32 [1], replicated, may hold values from 15360 to 16384
- step_lens: int32 [8], replicated, may hold values from 960 to 1024
Outputs:
- piece_out: bfloat16 [768, 4096], P('kv', 'tp')
- step_out: bfloat16 [8, 4096], P('kv', 'tp')
- piece_keys: bfloat16 [768, 8, 2, 128], P('kv', 'tp')
- piece_values: bfloat16 [768, 8, 256], P('kv', 'tp')
- step_keys: bfloat16 [8, 8, 2, 128], P('kv', 'tp')
- step_values: bfloat16 [8, 8, 256], P('kv', 'tp')
Inputs may be any that keep to these rules, and one draw needn't show every extreme that they name: `prompt_len`: the piece's tokens follow these cached positions. `step_lens`: each decoding token follows its sequence's cached positions.
All inputs are finite; a program needn't handle non-finite values.
Results may differ from a plain program's by a relative error of at most 0.015.
Values may be sent and summed in bfloat16 or wider, within the bound.
A program may use at most 128 MiB of HBM per device.

v0:
```python
import math

import jax
import jax.numpy as jnp
from jax import lax
from jax.sharding import PartitionSpec as P

EPS = 1e-06
OUT_SCALE = 0.8


def norm_rows(tokens, in_gain):
    floats = tokens.astype(jnp.float32)
    inv_rms = lax.rsqrt(jnp.mean(floats * floats, axis=-1, keepdims=True) + EPS)
    return (floats * inv_rms * in_gain).astype(jnp.bfloat16)


def project(normed, weight):
    flat_weight = weight.reshape(weight.shape[0], -1)
    product = jnp.dot(normed, flat_weight, preferred_element_type=jnp.float32)
    return product.astype(jnp.bfloat16).reshape((normed.shape[0],) + weight.shape[1:])


def piece_block(block_q, block_start, all_k, all_v, cache_ok, fresh_place):
    row_count = block_q.shape[0]
    row_place = block_start + jnp.arange(row_count, dtype=jnp.int32)
    visible = jnp.concatenate(
        [
            jnp.broadcast_to(cache_ok[None, :], (row_count, cache_ok.shape[0])),
            fresh_place[None, :] <= row_place[:, None],
        ],
        axis=1,
    )
    scores = jnp.einsum("qhcd,khcd->hcqk", block_q, all_k, preferred_element_type=jnp.float32)
    scores = scores * block_q.shape[-1] ** (-0.5)
    scores = jnp.where(visible[None, None], scores, -jnp.inf)
    maxima = jnp.max(scores, axis=-1)
    weights = jnp.exp(scores - maxima[..., None])
    totals = jnp.sum(weights, axis=-1)
    summed = jnp.einsum(
        "hcqk,khv->qhcv", weights.astype(jnp.bfloat16), all_v, preferred_element_type=jnp.float32
    )
    return (
        summed.astype(jnp.bfloat16),
        jnp.transpose(maxima, (2, 0, 1)),
        jnp.transpose(totals, (2, 0, 1)),
    )


def combine_parts(part_values, maxima, totals):
    row_best = jnp.max(maxima, axis=0)
    rescale = jnp.exp(maxima - row_best[None])
    return (
        jnp.sum(totals * rescale, axis=0),
        jnp.sum(part_values.astype(jnp.float32) * rescale[..., None], axis=0),
    )


def finish(norm_sum, value_sum, mix_ratio, out_gain):
    attended = value_sum / norm_sum[..., None]
    mixed = attended[:, :, 0] - mix_ratio[None, :, None] * attended[:, :, 1]
    inv_rms = lax.rsqrt(jnp.mean(mixed * mixed, axis=-1, keepdims=True) + EPS)
    return (mixed * inv_rms * out_gain[None, None, :] * OUT_SCALE).astype(jnp.bfloat16)


def on_device(
    piece_tokens,
    step_tokens,
    in_gain,
    w_query,
    w_key,
    w_value,
    w_out,
    mix_ratio,
    out_gain,
    prompt_keys,
    prompt_values,
    step_cache_keys,
    step_cache_values,
    prompt_len,
    step_lens,
):
    kv_place = lax.axis_index("kv")
    piece_dev = piece_tokens.shape[0]
    step_dev = step_tokens.shape[0]
    cache_dev = prompt_keys.shape[0]
    seq_count = step_cache_keys.shape[0]
    seq_cache = step_cache_keys.shape[1]
    all_rows = jnp.concatenate([piece_tokens, step_tokens], axis=0)
    normed = norm_rows(all_rows, in_gain)
    queries = project(normed, w_query)
    key_rows = project(normed, w_key)
    value_rows = project(normed, w_value)
    piece_k = key_rows[:piece_dev]
    step_k = key_rows[piece_dev:]
    piece_v = value_rows[:piece_dev]
    step_v = value_rows[piece_dev:]
    piece_q, step_q = (
        lax.all_gather(queries[:piece_dev], "kv", axis=0, tiled=True),
        lax.all_gather(queries[piece_dev:], "kv", axis=0, tiled=True),
    )
    all_k = jnp.concatenate([prompt_keys, piece_k], axis=0)
    all_v = jnp.concatenate([prompt_values, piece_v], axis=0)
    cache_ok = kv_place * cache_dev + jnp.arange(cache_dev, dtype=jnp.int32) < prompt_len[0]
    fresh_place = kv_place * piece_dev + jnp.arange(piece_dev, dtype=jnp.int32)
    piece_total = piece_q.shape[0]
    block_rows = math.gcd(piece_total, 512)
    blocks = piece_q.reshape((piece_total // block_rows, block_rows) + piece_q.shape[1:])
    starts = jnp.arange(piece_total // block_rows, dtype=jnp.int32) * block_rows

    def one_block(operands):
        return piece_block(operands[0], operands[1], all_k, all_v, cache_ok, fresh_place)

    summed, maxima, totals = lax.map(one_block, (blocks, starts))
    piece_sum = lax.optimization_barrier(summed.reshape((piece_total,) + summed.shape[2:]))
    piece_max = maxima.reshape((piece_total,) + maxima.shape[2:])
    piece_tot = totals.reshape((piece_total,) + totals.shape[2:])
    own_seq = jnp.arange(seq_count, dtype=jnp.int32) // step_dev == kv_place
    own_k = lax.dynamic_update_slice_in_dim(
        jnp.zeros((seq_count,) + step_k.shape[1:], jnp.bfloat16), step_k, kv_place * step_dev, 0
    )
    own_v = lax.dynamic_update_slice_in_dim(
        jnp.zeros((seq_count,) + step_v.shape[1:], jnp.bfloat16), step_v, kv_place * step_dev, 0
    )
    head_scale = step_q.shape[-1] ** (-0.5)
    cache_scores = (
        jnp.einsum("bhcd,bkhcd->bhck", step_q, step_cache_keys, preferred_element_type=jnp.float32)
        * head_scale
    )
    fresh_scores = (
        jnp.einsum("bhcd,bhcd->bhc", step_q, own_k, preferred_element_type=jnp.float32) * head_scale
    )
    cache_place = kv_place * seq_cache + jnp.arange(seq_cache, dtype=jnp.int32)
    cache_visible = cache_place[None, :] < step_lens[:, None]
    cache_scores = jnp.where(cache_visible[:, None, None, :], cache_scores, -jnp.inf)
    fresh_scores = jnp.where(own_seq[:, None, None], fresh_scores, -jnp.inf)
    step_max = jnp.maximum(jnp.max(cache_scores, axis=-1), fresh_scores)
    cache_weights = jnp.exp(cache_scores - step_max[..., None])
    fresh_weights = jnp.exp(fresh_scores - step_max)
    step_tot = jnp.sum(cache_weights, axis=-1) + fresh_weights
    fresh_rounded = lax.optimization_barrier(fresh_weights.astype(jnp.bfloat16))
    step_acc = jnp.einsum(
        "bhck,bkhv->bhcv",
        cache_weights.astype(jnp.bfloat16),
        step_cache_values,
        preferred_element_type=jnp.float32,
    )
    step_acc = (
        step_acc
        + fresh_rounded.astype(jnp.float32)[..., None] * own_v.astype(jnp.float32)[:, :, None, :]
    )
    step_sum = lax.optimization_barrier(step_acc.astype(jnp.bfloat16))
    value_parts = (
        lax.all_to_all(piece_sum[None], "kv", split_axis=1, concat_axis=0, tiled=True),
        lax.all_to_all(step_sum[None], "kv", split_axis=1, concat_axis=0, tiled=True),
    )
    stat_parts = (
        lax.all_to_all(piece_max[None], "kv", split_axis=1, concat_axis=0, tiled=True),
        lax.all_to_all(piece_tot[None], "kv", split_axis=1, concat_axis=0, tiled=True),
        lax.all_to_all(step_max[None], "kv", split_axis=1, concat_axis=0, tiled=True),
        lax.all_to_all(step_tot[None], "kv", split_axis=1, concat_axis=0, tiled=True),
    )
    piece_norm, piece_value = combine_parts(value_parts[0], stat_parts[0], stat_parts[1])
    step_norm, step_value = combine_parts(value_parts[1], stat_parts[2], stat_parts[3])
    headout = jnp.concatenate(
        [
            finish(piece_norm, piece_value, mix_ratio, out_gain),
            finish(step_norm, step_value, mix_ratio, out_gain),
        ],
        axis=0,
    )
    flat_heads = headout.reshape(headout.shape[0], -1)
    head_term = jnp.dot(
        flat_heads, w_out.reshape(-1, w_out.shape[-1]), preferred_element_type=jnp.float32
    ).astype(jnp.bfloat16)
    mixed = (
        lax.psum_scatter(head_term, "tp", scatter_dimension=1, tiled=True)
        .astype(jnp.float32)
        .astype(jnp.bfloat16)
    )
    return (mixed[:piece_dev], mixed[piece_dev:], piece_k, piece_v, step_k, step_v)


def solution(mesh):
    in_specs = (
        P("kv", None),
        P("kv", None),
        P(),
        P(None, "tp", None, None),
        P(None, "tp", None, None),
        P(None, "tp", None),
        P("tp", None, None),
        P("tp"),
        P(),
        P("kv", "tp", None, None),
        P("kv", "tp", None),
        P(None, "kv", "tp", None, None),
        P(None, "kv", "tp", None),
        P(),
        P(),
    )
    out_specs = (
        P("kv", "tp"),
        P("kv", "tp"),
        P("kv", "tp", None, None),
        P("kv", "tp", None),
        P("kv", "tp", None, None),
        P("kv", "tp", None),
    )
    return jax.shard_map(
        on_device, mesh=mesh, in_specs=in_specs, out_specs=out_specs, check_vma=False
    )
```

profile of v0, /device:TPU:0, one launch (start us, length us, event | category | flops | bytes accessed | tf_op | source)
XLA Modules:
  0.0 253.4 jit_solution(8422827475734836389)
XLA Ops:
  7.2 1.5 fusion.37
  8.8 7.3 %reshape.345 = bf16[4096,512]{1,0:T(8,128)(2,1)} reshape(bf16[4096,2,2,128]{3,2,1,0:T(2,128)(2,1)} %param.20) | data formatting | bytes 8388608 | tf_op jit(solution)/shard_map/reshape | solution.py:19
  16.1 3.0 %convolution_convert_fusion.2 = bf16[97,512]{1,0:T(8,128)(2,1)S(1)} fusion(bf16[4096,512]{1,0:T(8,128)(2,1)} %reshape.345, f32[4096]{0:T(1024)S(1)} %copy-done.27, f32[97]{0:T(128)S(1)} %add_rsqrt_fusion.2, bf16[1,4096]{1,0:T(2,128)(2,1)S(1)} %copy-done.19, bf16[96,4096]{1,0:T(8,128)(2,1)S(1)} %copy-done.7), kind=kOutput, calls=%fused_computation.42 | convolution fusion | flops 409678336 | bytes 5105028 | tf_op jit(solution)/shard_map/dot_general | solution.py:20
  19.1 22.3 %all_gather.7 = bf16[8,2,2,128]{3,2,1,0:T(2,128)(2,1)S(1)} all-gather(bf16[1,2,2,128]{3,2,1,0:T(2,128)(2,1)S(1)} %bitcast.154), channel_id=1, replica_groups=mesh['kv'=8,'tp'=4] {'kv'}, dimensions={0}, use_global_device_ids=true | all-gather | bytes 9216 | tf_op jit(solution)/shard_map/all_gather | solution.py:100
  41.4 7.2 %reshape.347 = bf16[4096,512]{1,0:T(8,128)(2,1)} reshape(bf16[4096,2,2,128]{3,2,1,0:T(2,128)(2,1)} %param.21) | data formatting | bytes 8388608 | tf_op jit(solution)/shard_map/reshape | solution.py:19
  48.7 3.1 %convolution_convert_fusion.1 = bf16[97,512]{1,0:T(8,128)(2,1)S(1)} fusion(bf16[4096,512]{1,0:T(8,128)(2,1)} %reshape.347, f32[4096]{0:T(1024)S(1)} %copy-done.27, f32[97]{0:T(128)S(1)} %add_rsqrt_fusion.2, bf16[1,4096]{1,0:T(2,128)(2,1)S(1)} %copy-done.19, bf16[96,4096]{1,0:T(8,128)(2,1)S(1)} %copy-done.7), kind=kOutput, calls=%fused_computation.41 | convolution fusion | flops 409678336 | bytes 5105028 | tf_op jit(solution)/shard_map/dot_general | solution.py:20
  52.7 0.7 fusion.62
  53.4 3.3 %all-to-all-start.4 = ((f32[1,8,2,2]{3,2,0,1:T(2,128)}), f32[1,8,2,2]{3,2,0,1:T(2,128)S(1)}, u32[]{:S(2)}, u32[]{:S(2)}) async-start(f32[1,8,2,2]{3,2,0,1:T(2,128)} %bitcast.38), calls=%async_computation.4 | async-start | bytes 16384 | tf_op jit(solution)/shard_map/all_to_all | solution.py:160
  56.7 0.9 fusion.52
  57.7 3.0 %copy.117 = bf16[512,8,2,256]{3,1,2,0:T(8,128)(2,1)S(1)} copy(bf16[512,8,2,256]{3,2,1,0:T(2,128)(2,1)} %bitcast.142) | data formatting | bytes 8388608
  60.8 1.5 convolution_convert_fusion
  62.2 1.4 add_bitcast_fusion
  63.7 34.9 %all_gather.6 = bf16[768,2,2,128]{3,0,2,1:T(8,128)(2,1)} all-gather(bf16[96,2,2,128]{3,0,2,1:T(8,128)(2,1)S(1)} %copy.69), channel_id=1, replica_groups=mesh['kv'=8,'tp'=4] {'kv'}, dimensions={0}, use_global_device_ids=true | all-gather | bytes 884736 | tf_op jit(solution)/shard_map/all_gather | solution.py:99
  98.7 1.6 copy.70
  101.1 1.6 copy.72
  102.6 1.9 pad_maximum_fusion
  104.9 1.5 pad_maximum_fusion.1
  106.4 38.5 %while.15 = (s32[]{:T(128)}, bf16[3,256,2,2,256]{4,1,0,3,2:T(8,128)(2,1)}, f32[3,256,2,2]{1,3,2,0:T(2,128)}, f32[3,256,2,2]{1,3,2,0:T(2,128)S(1)}, s32[3]{0:T(12...) while((s32[]{:T(128)}, ...), condition=%wide.region_4.5_spmd.clone, body=%wide.region_1.4_spmd.clone.sunk | while | flops 1711098240 | bytes 42593416 | solution.py:114
  108.4 2.0 pad_add_fusion.2
  110.4 2.5 %fusion.85 = (f32[2,2,256]{2,1,0:T(2,128)S(1)}, f32[2,2,256,2144]{2,3,1,0:T(8,128)S(1)}) fusion(pred[256,2144]{0,1:T(8,128)(4,1)S(1)} %pad_add_fusion.2, bf16[2144,2,2,128]{3,0,2,1:T(8,128)(2,1)S(1)} %get-tuple-element.265, bf16[3,256,2,2,128]{4,1,0,3,2:T(8,128)(2,1)} %get-tuple-element.264, s32[]{:T(128)S(6)} %copy.139), kind=kOutput, calls=%fused_computation.4.clone.1 | convolution fusion | flops 568622080 | bytes 11792388 | tf_op jit(solution)/shard_map/while/body/eval_jaxpr/qhcd,khcd->hcqk/dot_general | solution.py:34
  113.0 3.7 %fusion.86 = bf16[3,256,2,2,256]{4,1,0,3,2:T(8,128)(2,1)} fusion(bf16[3,256,2,2,256]{4,1,0,3,2:T(8,128)(2,1)} %get-tuple-element.247, s32[]{:T(128)S(6)} %copy.139, bf16[2144,2,256]{2,0,1:T(8,128)(2,1)S(1)} %copy-done.3, f32[2,2,256,2144]{2,3,1,0:T(8,128)S(1)} %get-tuple-element.229, f32[2,2,256]{2,1,0:T(2,128)S(1)} %get-tuple-element.230, ...), kind=kOutput, calls=%fused_computation.16.clone.1 | convolution fusion | flops 1133117440 | bytes 12054532 | tf_op jit(solution)/shard_map/while/body/eval_jaxpr/hcqk,khv->qhcv/dot_general | solution.py:40
  116.7 1.9 fusion.87
  121.2 2.0 pad_add_fusion.2
  123.3 2.6 %fusion.85 = (f32[2,2,256]{2,1,0:T(2,128)S(1)}, f32[2,2,256,2144]{2,3,1,0:T(8,128)S(1)}) fusion(pred[256,2144]{0,1:T(8,128)(4,1)S(1)} %pad_add_fusion.2, bf16[2144,2,2,128]{3,0,2,1:T(8,128)(2,1)S(1)} %get-tuple-element.265, bf16[3,256,2,2,128]{4,1,0,3,2:T(8,128)(2,1)} %get-tuple-element.264, s32[]{:T(128)S(6)} %copy.139), kind=kOutput, calls=%fused_computation.4.clone.1 | convolution fusion | flops 568622080 | bytes 11792388 | tf_op jit(solution)/shard_map/while/body/eval_jaxpr/qhcd,khcd->hcqk/dot_general | solution.py:34
  125.8 3.7 %fusion.86 = bf16[3,256,2,2,256]{4,1,0,3,2:T(8,128)(2,1)} fusion(bf16[3,256,2,2,256]{4,1,0,3,2:T(8,128)(2,1)} %get-tuple-element.247, s32[]{:T(128)S(6)} %copy.139, bf16[2144,2,256]{2,0,1:T(8,128)(2,1)S(1)} %copy-done.3, f32[2,2,256,2144]{2,3,1,0:T(8,128)S(1)} %get-tuple-element.229, f32[2,2,256]{2,1,0:T(2,128)S(1)} %get-tuple-element.230, ...), kind=kOutput, calls=%fused_computation.16.clone.1 | convolution fusion | flops 1133117440 | bytes 12054532 | tf_op jit(solution)/shard_map/while/body/eval_jaxpr/hcqk,khv->qhcv/dot_general | solution.py:40
  129.6 1.9 fusion.87
  134.0 2.0 pad_add_fusion.2
  136.1 2.6 %fusion.85 = (f32[2,2,256]{2,1,0:T(2,128)S(1)}, f32[2,2,256,2144]{2,3,1,0:T(8,128)S(1)}) fusion(pred[256,2144]{0,1:T(8,128)(4,1)S(1)} %pad_add_fusion.2, bf16[2144,2,2,128]{3,0,2,1:T(8,128)(2,1)S(1)} %get-tuple-element.265, bf16[3,256,2,2,128]{4,1,0,3,2:T(8,128)(2,1)} %get-tuple-element.264, s32[]{:T(128)S(6)} %copy.139), kind=kOutput, calls=%fused_computation.4.clone.1 | convolution fusion | flops 568622080 | bytes 11792388 | tf_op jit(solution)/shard_map/while/body/eval_jaxpr/qhcd,khcd->hcqk/dot_general | solution.py:34
  138.7 3.7 %fusion.86 = bf16[3,256,2,2,256]{4,1,0,3,2:T(8,128)(2,1)} fusion(bf16[3,256,2,2,256]{4,1,0,3,2:T(8,128)(2,1)} %get-tuple-element.247, s32[]{:T(128)S(6)} %copy.139, bf16[2144,2,256]{2,0,1:T(8,128)(2,1)S(1)} %copy-done.3, f32[2,2,256,2144]{2,3,1,0:T(8,128)S(1)} %get-tuple-element.229, f32[2,2,256]{2,1,0:T(2,128)S(1)} %get-tuple-element.230, ...), kind=kOutput, calls=%fused_computation.16.clone.1 | convolution fusion | flops 1133117440 | bytes 12054532 | tf_op jit(solution)/shard_map/while/body/eval_jaxpr/hcqk,khv->qhcv/dot_general | solution.py:40
  142.4 1.9 fusion.87
  144.8 0.7 slice_reduce_fusion
  145.6 5.3 %all-to-all-start.5 = ((f32[1,8,2,2]{3,2,0,1:T(2,128)}), f32[1,8,2,2]{3,2,0,1:T(2,128)S(1)}, u32[]{:S(2)}, u32[]{:S(2)}) async-start(f32[1,8,2,2]{3,2,0,1:T(2,128)} %add_bitcast_fusion), calls=%async_computation.5 | async-start | bytes 16384 | tf_op jit(solution)/shard_map/all_to_all | solution.py:161
  151.4 1.6 reshape.364
  153.0 4.4 %all-to-all-done.5 = f32[1,8,2,2]{3,2,0,1:T(2,128)S(1)} async-done(((f32[1,8,2,2]{3,2,0,1:T(2,128)}), f32[1,8,2,2]{3,2,0,1:T(2,128)S(1)}, u32[]{:S(2)}, u32[]{:S(2)}) %all-to-all-start.5) | async-done | bytes 160 | tf_op jit(solution)/shard_map/all_to_all | solution.py:161
  158.0 3.3 %all-to-all-start.2 = ((f32[8,1,384]{2,1,0:T(1,128)}), f32[8,1,384]{2,1,0:T(1,128)S(1)}, u32[]{:S(2)}, u32[]{:S(2)}) async-start(f32[8,1,384]{2,1,0:T(1,128)} %reshape.364), calls=%async_computation.2 | async-start | bytes 24576 | tf_op jit(solution)/shard_map/all_to_all | solution.py:159
  162.6 1.1 copy.104
  163.8 1.6 reshape.362
  165.4 2.5 all-to-all-done.2
  167.8 3.5 %all-to-all-start.1 = ((f32[8,1,384]{2,1,0:T(1,128)}), f32[8,1,384]{2,1,0:T(1,128)S(1)}, u32[]{:S(2)}, u32[]{:S(2)}) async-start(f32[8,1,384]{2,1,0:T(1,128)} %reshape.362), calls=%async_computation.1 | async-start | bytes 24576 | tf_op jit(solution)/shard_map/all_to_all | solution.py:158
  171.3 1.6 fusion.40
  173.0 4.9 %all-to-all-done.1 = f32[8,1,384]{2,1,0:T(1,128)S(1)} async-done(((f32[8,1,384]{2,1,0:T(1,128)}), f32[8,1,384]{2,1,0:T(1,128)S(1)}, u32[]{:S(2)}, u32[]{:S(2)}) %all-to-all-start.1) | async-done | bytes 12320 | tf_op jit(solution)/shard_map/all_to_all | solution.py:158
  177.9 3.6 %all-to-all-start.3 = ((bf16[1,8,2,2,256]{4,3,2,0,1:T(2,128)(2,1)}), bf16[1,8,2,2,256]{4,3,2,0,1:T(2,128)(2,1)S(1)}, u32[]{:S(2)}, u32[]{:S(2)}) async-start(bf16[1,8,2,2,256]{4,3,2,0,1:T(2,128)(2,1)} %bitcast.15), calls=%async_computation.3 | async-start | bytes 32768 | tf_op jit(solution)/shard_map/all_to_all | solution.py:155
  181.5 2.8 %copy.76 = bf16[1,768,2,2,256]{4,3,2,0,1:T(2,128)(2,1)} copy(bf16[1,768,2,2,256]{4,1,3,2,0:T(8,128)(2,1)S(1)} %bitcast.147) | data formatting | bytes 3145728 | tf_op jit(solution)/shard_map/broadcast_in_dim | solution.py:154
  184.2 3.6 %all-to-all-done.3 = bf16[1,8,2,2,256]{4,3,2,0,1:T(2,128)(2,1)S(1)} async-done(((bf16[1,8,2,2,256]{4,3,2,0,1:T(2,128)(2,1)}), bf16[1,8,2,2,256]{4,3,2,0,1:T(2,128)(2,1)S(1)}, u32[]{:S(2)}, u32[]{:S(2)}) %all-to-all-start.3) | async-done | bytes 16416 | tf_op jit(solution)/shard_map/all_to_all | solution.py:155
  187.8 4.1 %all-to-all-start = ((bf16[1,768,2,2,256]{4,3,2,0,1:T(2,128)(2,1)}), bf16[1,768,2,2,256]{4,3,2,0,1:T(2,128)(2,1)S(1)}, u32[]{:S(2)}, u32[]{:S(2)}) async-start(bf16[1,768,2,2,256]{4,3,2,0,1:T(2,128)(2,1)} %copy.76), calls=%async_computation | async-start | bytes 3145728 | tf_op jit(solution)/shard_map/all_to_all | solution.py:154
  192.2 0.7 copy.92
  193.0 0.7 fusion.60
  194.3 1.4 reduce.14
  195.6 1.1 reshape.363
  197.1 1.1 reduce_max.36
  198.2 1.3 reduce.13
  199.5 1.8 reshape.365
  201.6 1.0 copy.79
  202.7 0.8 fusion.49
  203.5 0.8 reshape_divide_fusion
  204.2 0.8 multiply_reduce_fusion.2
  205.0 0.8 multiply_convert_fusion.1
  205.8 10.1 %all-to-all-done = bf16[1,768,2,2,256]{4,3,2,0,1:T(2,128)(2,1)S(1)} async-done(((bf16[1,768,2,2,256]{4,3,2,0,1:T(2,128)(2,1)}), bf16[1,768,2,2,256]{4,3,2,0,1:T(2,128)(2,1)S(1)}, u32[]{:S(2)}, u32[]{:S(2)}) %all-to-all-start) | async-done | bytes 1572896 | tf_op jit(solution)/shard_map/all_to_all | solution.py:154
  215.9 1.1 convert.5
  218.0 1.2 copy-done.2
  219.2 1.7 fusion.35
  221.6 22.0 %reduce-scatter.2.cloned.1.call-done = bf16[97,1024]{1,0:T(8,128)(2,1)} async-done(((bf16[97,4096]{1,0:T(8,128)(2,1)}), bf16[97,1024]{1,0:T(8,128)(2,1)}) %reduce-scatter.2.cloned.1.call-update) | async-done | bytes 198672 | tf_op jit(solution)/shard_map/reduce_scatter | solution.py:177
  243.6 1.6 slice.82
  245.2 1.3 slice.83
  (131 shorter events, 15.4 us)
Async XLA Ops:
  7.2 164.2 %copy-start = (bf16[8,128,2,256]{3,2,1,0:T(2,128)(2,1)S(1)}, bf16[8,128,2,256]{3,2,1,0:T(2,128)(2,1)}, u32[]{:S(2)}) copy-start(bf16[8,128,2,256]{3,2,1,0:T(2,128)(2,1)} %param.29) | copy-start | bytes 3145732
  8.7 7.3 %copy-start.7 = (bf16[96,4096]{1,0:T(8,128)(2,1)S(1)}, bf16[96,4096]{1,0:T(8,128)(2,1)}, u32[]{:S(2)}) copy-start(bf16[96,4096]{1,0:T(8,128)(2,1)} %param.17) | copy-start | bytes 2359300
  8.7 7.3 %copy-start.19 = (bf16[1,4096]{1,0:T(2,128)(2,1)S(1)}, bf16[1,4096]{1,0:T(2,128)(2,1)}, u32[]{:S(2)}) copy-start(bf16[1,4096]{1,0:T(2,128)(2,1)} %param.18) | copy-start | bytes 24580
  8.8 7.3 %copy-start.27 = (f32[4096]{0:T(1024)S(1)}, f32[4096]{0:T(1024)}, u32[]{:S(2)}) copy-start(f32[4096]{0:T(1024)} %param.19) | copy-start | bytes 49156
  19.1 38.6 %copy-start.11 = (bf16[97,512]{1,0:T(8,128)(2,1)}, bf16[97,512]{1,0:T(8,128)(2,1)S(1)}, u32[]{:S(2)}) copy-start(bf16[97,512]{1,0:T(8,128)(2,1)S(1)} %convolution_convert_fusion.2) | copy-start | bytes 297988
  48.6 3.2 %copy-start.26 = (bf16[8,128,2,2,128]{4,3,2,1,0:T(2,128)(2,1)S(1)}, bf16[8,128,2,2,128]{4,3,2,1,0:T(2,128)(2,1)}, u32[]{:S(2)}) copy-start(bf16[8,128,2,2,128]{4,3,2,1,0:T(2,128)(2,1)} %param.28) | copy-start | bytes 3145732
  48.6 3.8 %copy-start.25 = (s32[8]{0:T(128)S(1)}, s32[8]{0:T(128)}, u32[]{:S(2)}) copy-start(s32[8]{0:T(128)} %param.31) | copy-start | bytes 100
  51.8 8.9 %copy-start.10 = (bf16[97,512]{1,0:T(8,128)(2,1)}, bf16[97,512]{1,0:T(8,128)(2,1)S(1)}, u32[]{:S(2)}) copy-start(bf16[97,512]{1,0:T(8,128)(2,1)S(1)} %convolution_convert_fusion.1) | copy-start | bytes 297988
  51.8 1.6 copy-start.23
  53.4 92.2 %all-to-all-start.4 = ((f32[1,8,2,2]{3,2,0,1:T(2,128)}), f32[1,8,2,2]{3,2,0,1:T(2,128)S(1)}, u32[]{:S(2)}, u32[]{:S(2)}) async-start(f32[1,8,2,2]{3,2,0,1:T(2,128)} %bitcast.38), calls=%async_computation.4 | async-start | bytes 16384 | tf_op jit(solution)/shard_map/all_to_all | solution.py:160
  57.7 3.0 %copy-start.8 = (bf16[96,4096]{1,0:T(8,128)(2,1)S(1)}, bf16[96,4096]{1,0:T(8,128)(2,1)}, u32[]{:S(2)}) copy-start(bf16[96,4096]{1,0:T(8,128)(2,1)} %param.17) | copy-start | bytes 2359300
  57.7 3.0 %copy-start.28 = (f32[4096]{0:T(1024)S(1)}, f32[4096]{0:T(1024)}, u32[]{:S(2)}) copy-start(f32[4096]{0:T(1024)} %param.19) | copy-start | bytes 49156
  60.7 2.9 %slice-start.1 = ((bf16[97,512]{1,0:T(8,128)(2,1)}), bf16[96,512]{1,0:T(8,128)(2,1)S(1)}, s32[]{:S(2)}) async-start(bf16[97,512]{1,0:T(8,128)(2,1)} %copy-done.11), calls=%async_computation.9 | async-start | bytes 196608 | tf_op jit(solution)/shard_map/slice | solution.py:99
  60.7 37.8 %slice-start = ((bf16[97,512]{1,0:T(8,128)(2,1)}), bf16[96,512]{1,0:T(8,128)(2,1)S(1)}, s32[]{:S(2)}) async-start(bf16[97,512]{1,0:T(8,128)(2,1)} %copy-done.10), calls=%async_computation.8 | async-start | bytes 196608 | tf_op jit(solution)/shard_map/slice | solution.py:94
  60.8 37.9 %copy-start.4 = (bf16[2048,2,2,128]{3,2,1,0:T(2,128)(2,1)S(1)}, bf16[2048,2,2,128]{3,2,1,0:T(2,128)(2,1)}, u32[]{:S(2)}) copy-start(bf16[2048,2,2,128]{3,2,1,0:T(2,128)(2,1)} %param.26) | copy-start | bytes 6291460
  98.6 1.7 copy-start.9
  98.6 1.7 copy-start.13
  98.7 2.4 copy-start.5
  102.6 2.2 copy-start.1
  102.6 2.2 copy-start.12
  104.9 1.5 copy-start.20
  110.4 2.6 %copy-start.3 = (bf16[2144,2,256]{2,0,1:T(8,128)(2,1)S(1)}, bf16[2144,2,256]{2,0,1:T(8,128)(2,1)}, u32[]{:S(2)}) copy-start(bf16[2144,2,256]{2,0,1:T(8,128)(2,1)} %get-tuple-element.266) | copy-start | bytes 6586372 | tf_op jit(solution)/shard_map/while
  123.2 2.6 %copy-start.3 = (bf16[2144,2,256]{2,0,1:T(8,128)(2,1)S(1)}, bf16[2144,2,256]{2,0,1:T(8,128)(2,1)}, u32[]{:S(2)}) copy-start(bf16[2144,2,256]{2,0,1:T(8,128)(2,1)} %get-tuple-element.266) | copy-start | bytes 6586372 | tf_op jit(solution)/shard_map/while
  136.1 2.6 %copy-start.3 = (bf16[2144,2,256]{2,0,1:T(8,128)(2,1)S(1)}, bf16[2144,2,256]{2,0,1:T(8,128)(2,1)}, u32[]{:S(2)}) copy-start(bf16[2144,2,256]{2,0,1:T(8,128)(2,1)} %get-tuple-element.266) | copy-start | bytes 6586372 | tf_op jit(solution)/shard_map/while
  145.6 27.4 %copy-start.24 = (bf16[1,2,256]{2,1,0:T(2,128)(2,1)}, bf16[1,2,256]{2,1,0:T(2,128)(2,1)S(1)}, u32[]{:S(2)}) copy-start(bf16[1,2,256]{2,1,0:T(2,128)(2,1)S(1)} %slice.67) | copy-start | bytes 3076
  145.6 11.8 %all-to-all-start.5 = ((f32[1,8,2,2]{3,2,0,1:T(2,128)}), f32[1,8,2,2]{3,2,0,1:T(2,128)S(1)}, u32[]{:S(2)}, u32[]{:S(2)}) async-start(f32[1,8,2,2]{3,2,0,1:T(2,128)} %add_bitcast_fusion), calls=%async_computation.5 | async-start | bytes 16384 | tf_op jit(solution)/shard_map/all_to_all | solution.py:161
  151.4 30.1 %copy-start.6 = (bf16[3,256,2,2,256]{4,1,0,3,2:T(8,128)(2,1)S(1)}, bf16[3,256,2,2,256]{4,1,0,3,2:T(8,128)(2,1)}, u32[]{:S(2)}) copy-start(bf16[3,256,2,2,256]{4,1,0,3,2:T(8,128)(2,1)} %get-tuple-element.60) | copy-start | bytes 4718596
  157.4 0.6 copy-start.17
  158.0 9.8 %all-to-all-start.2 = ((f32[8,1,384]{2,1,0:T(1,128)}), f32[8,1,384]{2,1,0:T(1,128)S(1)}, u32[]{:S(2)}, u32[]{:S(2)}) async-start(f32[8,1,384]{2,1,0:T(1,128)} %reshape.364), calls=%async_computation.2 | async-start | bytes 24576 | tf_op jit(solution)/shard_map/all_to_all | solution.py:159
  167.8 10.0 %copy-start.14 = (f32[8,1,384]{2,1,0:T(1,128)}, f32[8,1,384]{2,1,0:T(1,128)S(1)}, u32[]{:S(2)}) copy-start(f32[8,1,384]{2,1,0:T(1,128)S(1)} %all-to-all-done.2) | copy-start | bytes 36868
  167.8 10.0 %all-to-all-start.1 = ((f32[8,1,384]{2,1,0:T(1,128)}), f32[8,1,384]{2,1,0:T(1,128)S(1)}, u32[]{:S(2)}, u32[]{:S(2)}) async-start(f32[8,1,384]{2,1,0:T(1,128)} %reshape.362), calls=%async_computation.1 | async-start | bytes 24576 | tf_op jit(solution)/shard_map/all_to_all | solution.py:158
  177.9 10.0 %copy-start.16 = (f32[8,1,384]{2,1,0:T(1,128)}, f32[8,1,384]{2,1,0:T(1,128)S(1)}, u32[]{:S(2)}) copy-start(f32[8,1,384]{2,1,0:T(1,128)S(1)} %all-to-all-done.1) | copy-start | bytes 36868
  177.9 10.0 %all-to-all-start.3 = ((bf16[1,8,2,2,256]{4,3,2,0,1:T(2,128)(2,1)}), bf16[1,8,2,2,256]{4,3,2,0,1:T(2,128)(2,1)S(1)}, u32[]{:S(2)}, u32[]{:S(2)}) async-start(bf16[1,8,2,2,256]{4,3,2,0,1:T(2,128)(2,1)} %bitcast.15), calls=%async_computation.3 | async-start | bytes 32768 | tf_op jit(solution)/shard_map/all_to_all | solution.py:155
  184.2 8.7 %copy-start.18 = (f32[1,8,2,2]{3,2,0,1:T(2,128)S(1)}, f32[1,8,2,2]{3,2,0,1:T(2,128)}, u32[]{:S(2)}) copy-start(f32[1,8,2,2]{3,2,0,1:T(2,128)} %copy-done.17) | copy-start | bytes 388
  184.2 14.0 %copy-start.15 = (f32[8,1,384]{2,1,0:T(1,128)S(1)}, f32[8,1,384]{2,1,0:T(1,128)}, u32[]{:S(2)}) copy-start(f32[8,1,384]{2,1,0:T(1,128)} %copy-done.14) | copy-start | bytes 36868
  187.8 28.0 %all-to-all-start = ((bf16[1,768,2,2,256]{4,3,2,0,1:T(2,128)(2,1)}), bf16[1,768,2,2,256]{4,3,2,0,1:T(2,128)(2,1)S(1)}, u32[]{:S(2)}, u32[]{:S(2)}) async-start(bf16[1,768,2,2,256]{4,3,2,0,1:T(2,128)(2,1)} %copy.76), calls=%async_computation | async-start | bytes 3145728 | tf_op jit(solution)/shard_map/all_to_all | solution.py:154
  192.0 51.6 %reduce-scatter.2.cloned.1.call-start = ((), (), s32[]{:S(2)}) async-start(), calls=%async_computation.7 | async-start | bytes 1064960 | tf_op jit(solution)/shard_map/reduce_scatter | solution.py:177
  217.0 0.7 copy-start.21
  217.0 0.9 copy-start.22
  217.0 2.2 copy-start.2
Sparse Core Ops, SparseCore 0:
  221.0 22.5 reduce-scatter.1
where the time goes:
time: 255 us; the launch traced here: 253 us
  blocking collectives  57.2 us (22%)
  waiting for transfers between devices  47.5 us (19%)
  local copies, waits for them, and re-layouts  45.4 us (18%)
  other arithmetic  35 us (14%)
  matrix products  30.4 us (12%)
  starting transfers between devices  23.2 us (9%)
  between operations  14.5 us (6%)
    all_gather x1, blocking collectives, on_device(): lax.all_gather(queries[:piece_dev], 'kv', axis=0, tiled=True)  34.9 us
    all_gather x1, blocking collectives, on_device(): lax.all_gather(queries[piece_dev:], 'kv', axis=0, tiled=True)  22.3 us
    reduce_scatter x1, waiting for transfers between devices, on_device(): lax.psum_scatter(head_term, 'tp', scatter_dimension=1, tiled=True)  22 us
    unnamed x63, local copies, waits for them, and re-layouts  14.8 us
    reshape x2, local copies, waits for them, and re-layouts, project(): flat_weight = weight.reshape(weight.shape[0], -1)  14.5 us
    dot_general x3, matrix products, piece_block(): jnp.einsum('hcqk,khv->qhcv', weights.astype(jnp.bfloat16), all_v, preferr...  11.2 us
    all_to_all x1, waiting for transfers between devices, on_device(): lax.all_to_all(piece_sum[None], 'kv', split_axis=1, concat_axis=0, tiled=...  10.1 us
    dot_general x3, matrix products, piece_block(): jnp.einsum('qhcd,khcd->hcqk', block_q, all_k, preferred_element_type=jnp....  7.65 us
  transfers between devices with their start and end apart: 7, of which 6 were waited for; matrix products, arithmetic and copies ran while one was open for 31% of the time, Pallas kernels for 0%

commit v1 on v0

v1 whole, which is shorter than its diff:
```python
import functools
import math

import jax
import jax.numpy as jnp
from jax import lax
from jax.experimental import pallas as pl
from jax.experimental.pallas import tpu as pltpu
from jax.sharding import PartitionSpec as P

EPS = 1e-06
OUT_SCALE = 0.8
MESH = pl.DeviceIdType.MESH
HIDDEN = -1e30


def norm_rows(tokens, in_gain):
    floats = tokens.astype(jnp.float32)
    inv_rms = lax.rsqrt(jnp.mean(floats * floats, axis=-1, keepdims=True) + EPS)
    return (floats * inv_rms * in_gain).astype(jnp.bfloat16)


def project(normed, weight):
    order = tuple(range(1, weight.ndim - 1)) + (0, weight.ndim - 1)
    parts = jnp.transpose(weight, order)
    parts = parts.reshape((-1,) + parts.shape[-2:])
    product = jnp.einsum("nd,gdk->gnk", normed, parts, preferred_element_type=jnp.float32)
    return product.astype(jnp.bfloat16)


def meet(axis, count):
    me = lax.axis_index(axis)
    barrier = pltpu.get_barrier_semaphore()
    for step in range(1, count):
        pl.semaphore_signal(
            barrier, inc=1, device_id={axis: lax.rem(me + step, count)}, device_id_type=MESH
        )
    pl.semaphore_wait(barrier, count - 1)
    return me


def gather_kernel(axis, count, own, everyone, send_sem, recv_sem):
    me = meet(axis, count)
    copies = []
    for step in range(1, count):
        copy = pltpu.make_async_remote_copy(
            src_ref=own,
            dst_ref=everyone.at[me],
            send_sem=send_sem.at[step],
            recv_sem=recv_sem.at[step],
            device_id={axis: lax.rem(me + step, count)},
            device_id_type=MESH,
        )
        copy.start()
        copies.append(copy)
    everyone[me] = own[...]
    for copy in copies:
        copy.wait()


def gather_rows(own, axis, count, collective):
    return pl.pallas_call(
        functools.partial(gather_kernel, axis, count),
        out_shape=jax.ShapeDtypeStruct((count,) + own.shape, own.dtype),
        in_specs=[pl.BlockSpec(memory_space=pltpu.VMEM)],
        out_specs=pl.BlockSpec(memory_space=pltpu.VMEM),
        scratch_shapes=[
            pltpu.SemaphoreType.DMA((count,)),
            pltpu.SemaphoreType.DMA((count,)),
        ],
        compiler_params=pltpu.CompilerParams(collective_id=collective, has_side_effects=True),
        name="gather_rows",
    )(own)


def attend_kernel(rows, dims, q_ref, k_ref, v_ref, fk_ref, fv_ref, bias_ref, own_ref, o_ref, s_ref):
    part = pl.program_id(1)
    owners = q_ref.shape[0]
    scale = dims ** (-0.5)
    fold = scale * math.log2(math.e)
    q = q_ref[:, :rows, :].reshape(owners * rows, dims)
    contract = (((1,), (1,)), ((), ()))
    old = lax.dot_general(q, k_ref[0], contract, preferred_element_type=jnp.float32)
    old = old + bias_ref[...]
    new = lax.dot_general(q, fk_ref[0], contract, preferred_element_type=jnp.float32)
    place = pl.program_id(0) * owners * rows + lax.broadcasted_iota(jnp.int32, new.shape, 0)
    new = jnp.where(own_ref[...] <= place, new, HIDDEN)
    top = jnp.maximum(
        jnp.max(old, axis=1, keepdims=True), jnp.max(new, axis=1, keepdims=True)
    )
    old_w = jnp.exp2((old - top) * fold)
    new_w = jnp.exp2((new - top) * fold)
    total = jnp.sum(old_w, axis=1, keepdims=True) + jnp.sum(new_w, axis=1, keepdims=True)
    summed = jnp.dot(old_w.astype(jnp.bfloat16), v_ref[0], preferred_element_type=jnp.float32)
    summed += jnp.dot(new_w.astype(jnp.bfloat16), fv_ref[0], preferred_element_type=jnp.float32)
    o_ref[...] = summed.astype(jnp.bfloat16).reshape(o_ref.shape)
    parts = pl.num_programs(1)
    lane = lax.broadcasted_iota(jnp.int32, (owners * rows, s_ref.shape[-1]), 1)
    put = jnp.where(lane == part, top * scale, jnp.where(lane == parts + part, total, 0.0))
    put = put.reshape(s_ref.shape)

    @pl.when(part == 0)
    def _():
        s_ref[...] = put

    @pl.when(part != 0)
    def _():
        s_ref[...] += put


def attend(q_all, keys, values, fresh_k, fresh_v, bias, fresh_place, rows):
    count, padded, _ = q_all.shape
    parts, cached, dims = keys.shape
    maps = parts // values.shape[0]
    wide = values.shape[-1]
    owners = math.gcd(count, 2)
    return pl.pallas_call(
        functools.partial(attend_kernel, rows, dims),
        grid=(count // owners, parts),
        in_specs=[
            pl.BlockSpec((owners, padded, dims), lambda i, p: (i, 0, p)),
            pl.BlockSpec((1, cached, dims), lambda i, p: (p, 0, 0)),
            pl.BlockSpec((1, cached, wide), lambda i, p: (p // maps, 0, 0)),
            pl.BlockSpec((1, rows, dims), lambda i, p: (p, 0, 0)),
            pl.BlockSpec((1, rows, wide), lambda i, p: (p // maps, 0, 0)),
            pl.BlockSpec((1, cached), lambda i, p: (0, 0)),
            pl.BlockSpec((1, rows), lambda i, p: (0, 0)),
        ],
        out_specs=[
            pl.BlockSpec((owners, rows, wide), lambda i, p: (i, 0, p)),
            pl.BlockSpec((owners, rows, 128), lambda i, p: (i, 0, 0)),
        ],
        out_shape=[
            jax.ShapeDtypeStruct((count, rows, parts * wide), jnp.bfloat16),
            jax.ShapeDtypeStruct((count, rows, 128), jnp.float32),
        ],
        compiler_params=pltpu.CompilerParams(
            dimension_semantics=("arbitrary", "arbitrary"), vmem_limit_bytes=56 * 1024 * 1024
        ),
        name="attend",
    )(q_all, keys, values, fresh_k, fresh_v, bias, fresh_place)


def mix_maps(first, second, ratio, gain):
    mixed = first - ratio * second
    inv_rms = lax.rsqrt(jnp.mean(mixed * mixed, axis=-1, keepdims=True) + EPS)
    return (mixed * inv_rms * gain * OUT_SCALE).astype(jnp.bfloat16)


def blend(values, tops, totals):
    count = len(values)
    best = functools.reduce(jnp.maximum, tops)
    scales = [jnp.exp(top - best) for top in tops]
    norm = functools.reduce(jnp.add, [scales[g] * totals[g] for g in range(count)])
    total = functools.reduce(jnp.add, [values[g] * scales[g] for g in range(count)])
    return total / norm


def exchange_kernel(
    axis, count, parts, maps, wide, ratio, gain, vals, stats, step, out, all_v, all_s, all_t, send_sem, recv_sem
):
    me = meet(axis, count)
    copies = []
    for turn in range(1, count):
        other = lax.rem(me + turn, count)
        for slot, (mine, theirs) in enumerate(((stats, all_s), (step, all_t), (vals, all_v))):
            copy = pltpu.make_async_remote_copy(
                src_ref=mine.at[other],
                dst_ref=theirs.at[me],
                send_sem=send_sem.at[turn, slot],
                recv_sem=recv_sem.at[turn, slot],
                device_id={axis: other},
                device_id_type=MESH,
            )
            copy.start()
            copies.append(copy)
    all_v[me] = vals[me]
    all_s[me] = stats[me]
    all_t[me] = step[me]
    for copy in copies:
        copy.wait()
    rows = vals.shape[1]
    steps = step.shape[1] // parts
    out[...] = jnp.zeros_like(out)
    tall = math.gcd(rows, 32)

    def chunk(index, carry):
        at = pl.ds(pl.multiple_of(index * tall, tall), tall)
        for head in range(parts // maps):
            maps_out = []
            for part in range(head * maps, head * maps + maps):
                cut = slice(part * wide, part * wide + wide)
                maps_out.append(
                    blend(
                        [all_v[g, at, cut].astype(jnp.float32) for g in range(count)],
                        [all_s[g, at, part : part + 1] for g in range(count)],
                        [all_s[g, at, parts + part : parts + part + 1] for g in range(count)],
                    )
                )
            out[at, head * wide : head * wide + wide] = mix_maps(
                maps_out[0], maps_out[1], ratio[0, head], gain[...]
            )
        return carry

    lax.fori_loop(0, rows // tall, chunk, 0)
    low = out.shape[0] - rows
    for head in range(parts // maps):
        lines = []
        for seq in range(steps):
            maps_out = []
            for part in range(seq * parts + head * maps, seq * parts + head * maps + maps):
                line = [all_t[g, part : part + 1, :] for g in range(count)]
                maps_out.append(
                    blend(
                        [v[:, :wide] for v in line],
                        [v[:, wide : wide + 1] for v in line],
                        [v[:, wide + 1 : wide + 2] for v in line],
                    )
                )
            lines.append(mix_maps(maps_out[0], maps_out[1], ratio[0, head], gain[...]).astype(jnp.float32))
        place = lax.broadcasted_iota(jnp.int32, (low, wide), 0)
        block = jnp.zeros((low, wide), jnp.float32)
        for seq in range(steps):
            block = jnp.where(place == seq, lines[seq], block)
        out[rows:, head * wide : head * wide + wide] = block.astype(jnp.bfloat16)


def exchange(values, stats, step, ratio, gain, axis, count, maps, padded, collective):
    parts = values.shape[-1] // gain.shape[-1]
    wide = gain.shape[-1]
    vmem = pl.BlockSpec(memory_space=pltpu.VMEM)
    return pl.pallas_call(
        functools.partial(exchange_kernel, axis, count, parts, maps, wide),
        out_shape=jax.ShapeDtypeStruct((padded, parts // maps * wide), jnp.bfloat16),
        in_specs=[pl.BlockSpec(memory_space=pltpu.SMEM), vmem, vmem, vmem, vmem],
        out_specs=vmem,
        scratch_shapes=[
            pltpu.VMEM(values.shape, values.dtype),
            pltpu.VMEM(stats.shape, stats.dtype),
            pltpu.VMEM(step.shape, step.dtype),
            pltpu.SemaphoreType.DMA((count, 3)),
            pltpu.SemaphoreType.DMA((count, 3)),
        ],
        compiler_params=pltpu.CompilerParams(
            collective_id=collective, has_side_effects=True, vmem_limit_bytes=56 * 1024 * 1024
        ),
        name="exchange",
    )(ratio, gain, values, stats, step)


def project_out_kernel(axis, count, heads, weight, out, terms, pair, half, far, d_send, d_recv, x_send, x_recv):
    me = lax.axis_index(axis)
    chips = count // 2
    chip, core = me // 2, lax.rem(me, 2)
    meet(axis, count)
    wide = out.shape[1]
    for target in range(count):
        terms[target] = jnp.dot(
            heads[...], weight[:, target * wide : target * wide + wide], preferred_element_type=jnp.float32
        ).astype(jnp.bfloat16)
    near = []
    for turn in range(1, chips + 1):
        there = lax.rem(chip + turn, chips)
        copy = pltpu.make_async_remote_copy(
            src_ref=terms.at[there * 2 + 1 - core],
            dst_ref=pair.at[there],
            send_sem=d_send.at[turn],
            recv_sem=d_recv.at[turn],
            device_id={axis: chip * 2 + 1 - core},
            device_id_type=MESH,
        )
        copy.start()
        near.append(copy)
    away = []
    for turn in range(1, chips + 1):
        near[turn - 1].wait()
        there = lax.rem(chip + turn, chips)
        both = terms[there * 2 + core].astype(jnp.float32) + pair[there].astype(jnp.float32)
        if turn == chips:
            total = both
            for copy in away:
                copy.wait()
            for slot in range(1, chips):
                total = total + far[slot].astype(jnp.float32)
            out[...] = total.astype(jnp.bfloat16)
        else:
            half[turn] = both.astype(jnp.bfloat16)
            copy = pltpu.make_async_remote_copy(
                src_ref=half.at[turn],
                dst_ref=far.at[turn],
                send_sem=x_send.at[turn],
                recv_sem=x_recv.at[turn],
                device_id={axis: there * 2 + core},
                device_id_type=MESH,
            )
            copy.start()
            away.append(copy)


def project_out(heads, weight, axis, count, collective):
    wide = weight.shape[1] // count
    rows = heads.shape[0]
    chips = count // 2
    vmem = pl.BlockSpec(memory_space=pltpu.VMEM)
    return pl.pallas_call(
        functools.partial(project_out_kernel, axis, count),
        out_shape=jax.ShapeDtypeStruct((rows, wide), jnp.bfloat16),
        in_specs=[vmem, vmem],
        out_specs=vmem,
        scratch_shapes=[
            pltpu.VMEM((count, rows, wide), jnp.bfloat16),
            pltpu.VMEM((chips, rows, wide), jnp.bfloat16),
            pltpu.VMEM((chips, rows, wide), jnp.bfloat16),
            pltpu.VMEM((chips, rows, wide), jnp.bfloat16),
            pltpu.SemaphoreType.DMA((chips + 1,)),
            pltpu.SemaphoreType.DMA((chips + 1,)),
            pltpu.SemaphoreType.DMA((chips + 1,)),
            pltpu.SemaphoreType.DMA((chips + 1,)),
        ],
        compiler_params=pltpu.CompilerParams(
            collective_id=collective, has_side_effects=True, vmem_limit_bytes=56 * 1024 * 1024
        ),
        name="project_out",
    )(heads, weight)


def on_device(
    kv_count,
    tp_count,
    piece_tokens,
    step_tokens,
    in_gain,
    w_query,
    w_key,
    w_value,
    w_out,
    mix_ratio,
    out_gain,
    prompt_keys,
    prompt_values,
    step_cache_keys,
    step_cache_values,
    prompt_len,
    step_lens,
):
    kv_place = lax.axis_index("kv")
    piece_dev = piece_tokens.shape[0]
    step_dev = step_tokens.shape[0]
    cache_dev = prompt_keys.shape[0]
    seq_count = step_cache_keys.shape[0]
    seq_cache = step_cache_keys.shape[1]
    heads, maps, dims = w_query.shape[1:]
    wide = w_value.shape[-1]
    parts = heads * maps
    padded = -(-(piece_dev + step_dev) // 16) * 16
    spare = jnp.zeros((padded - piece_dev - step_dev, piece_tokens.shape[1]), jnp.bfloat16)
    all_rows = jnp.concatenate([piece_tokens, step_tokens, spare], axis=0)
    normed = norm_rows(all_rows, in_gain)
    queries = project(normed, w_query)
    key_rows = project(normed, w_key)
    value_rows = project(normed, w_value)
    q_flat = jnp.transpose(queries, (1, 0, 2)).reshape(padded, parts * dims)
    q_all = gather_rows(q_flat, "kv", kv_count, 0)
    end = piece_dev + step_dev

    def rows_of(flat, start, stop, extra):
        return jnp.transpose(flat[:, start:stop], (1, 0, 2)).reshape((stop - start,) + extra)

    piece_k = rows_of(key_rows, 0, piece_dev, (heads, maps, dims))
    step_k = rows_of(key_rows, piece_dev, end, (heads, maps, dims))
    piece_v = rows_of(value_rows, 0, piece_dev, (heads, wide))
    step_v = rows_of(value_rows, piece_dev, end, (heads, wide))
    keys = jnp.transpose(prompt_keys, (1, 2, 0, 3)).reshape(parts, cache_dev, dims)
    values = jnp.transpose(prompt_values, (1, 0, 2))
    cache_ok = kv_place * cache_dev + jnp.arange(cache_dev, dtype=jnp.int32) < prompt_len[0]
    bias = jnp.where(cache_ok, 0.0, HIDDEN)[None, :]
    fresh_place = (kv_place * piece_dev + jnp.arange(piece_dev, dtype=jnp.int32))[None, :]
    piece_sum, piece_stats = attend(
        q_all,
        keys,
        values,
        key_rows[:, :piece_dev],
        value_rows[:, :piece_dev],
        bias,
        fresh_place,
        piece_dev,
    )
    step_q = q_all[:, piece_dev:end].reshape(seq_count, heads, maps, dims)
    own_seq = jnp.arange(seq_count, dtype=jnp.int32) // step_dev == kv_place
    own_k = lax.dynamic_update_slice_in_dim(
        jnp.zeros((seq_count,) + step_k.shape[1:], jnp.bfloat16), step_k, kv_place * step_dev, 0
    )
    own_v = lax.dynamic_update_slice_in_dim(
        jnp.zeros((seq_count,) + step_v.shape[1:], jnp.bfloat16), step_v, kv_place * step_dev, 0
    )
    head_scale = step_q.shape[-1] ** (-0.5)
    cache_scores = (
        jnp.einsum("bhcd,bkhcd->bhck", step_q, step_cache_keys, preferred_element_type=jnp.float32)
        * head_scale
    )
    fresh_scores = (
        jnp.einsum("bhcd,bhcd->bhc", step_q, own_k, preferred_element_type=jnp.float32) * head_scale
    )
    cache_place = kv_place * seq_cache + jnp.arange(seq_cache, dtype=jnp.int32)
    cache_visible = cache_place[None, :] < step_lens[:, None]
    cache_scores = jnp.where(cache_visible[:, None, None, :], cache_scores, -jnp.inf)
    fresh_scores = jnp.where(own_seq[:, None, None], fresh_scores, -jnp.inf)
    step_max = jnp.maximum(jnp.max(cache_scores, axis=-1), fresh_scores)
    cache_weights = jnp.exp(cache_scores - step_max[..., None])
    fresh_weights = jnp.exp(fresh_scores - step_max)
    step_tot = jnp.sum(cache_weights, axis=-1) + fresh_weights
    fresh_rounded = lax.optimization_barrier(fresh_weights.astype(jnp.bfloat16))
    step_acc = jnp.einsum(
        "bhck,bkhv->bhcv",
        cache_weights.astype(jnp.bfloat16),
        step_cache_values,
        preferred_element_type=jnp.float32,
    )
    step_acc = (
        step_acc
        + fresh_rounded.astype(jnp.float32)[..., None] * own_v.astype(jnp.float32)[:, :, None, :]
    )
    step_sum = lax.optimization_barrier(step_acc.astype(jnp.bfloat16))
    message = jnp.concatenate(
        [
            step_sum.astype(jnp.float32),
            step_max[..., None],
            step_tot[..., None],
            jnp.zeros(step_tot.shape + (126,), jnp.float32),
        ],
        axis=-1,
    ).reshape(kv_count, step_dev * parts, wide + 128)
    flat_heads = exchange(
        piece_sum,
        piece_stats,
        message,
        mix_ratio[None, :],
        out_gain[None, :],
        "kv",
        kv_count,
        maps,
        padded,
        1,
    )
    mixed = project_out(flat_heads, w_out.reshape(-1, w_out.shape[-1]), "tp", tp_count, 2)
    return (mixed[:piece_dev], mixed[piece_dev:end], piece_k, piece_v, step_k, step_v)


def solution(mesh):
    in_specs = (
        P("kv", None),
        P("kv", None),
        P(),
        P(None, "tp", None, None),
        P(None, "tp", None, None),
        P(None, "tp", None),
        P("tp", None, None),
        P("tp"),
        P(),
        P("kv", "tp", None, None),
        P("kv", "tp", None),
        P(None, "kv", "tp", None, None),
        P(None, "kv", "tp", None),
        P(),
        P(),
    )
    out_specs = (
        P("kv", "tp"),
        P("kv", "tp"),
        P("kv", "tp", None, None),
        P("kv", "tp", None),
        P("kv", "tp", None, None),
        P("kv", "tp", None),
    )
    return jax.shard_map(
        functools.partial(on_device, mesh.shape["kv"], mesh.shape["tp"]),
        mesh=mesh, in_specs=in_specs, out_specs=out_specs, check_vma=False
    )
```

time: 255 us -> 143 us (0.56)
  the two profiles are of different devices: /device:TPU:0 before, /device:TPU:12 now
where the time goes in v1:
time: 143 us
  Pallas kernels  116 us (81%)
  local copies, waits for them, and re-layouts  12.8 us (9%)
  matrix products  8.35 us (6%)
  other arithmetic  4.02 us (3%)
  between operations  1.57 us (1%)
    pallas_call x1, Pallas kernels, exchange(): pl.pallas_call(functools.partial(exchange_kernel, axis, count, parts, map...  51.1 us
    pallas_call x1, Pallas kernels, gather_rows(): pl.pallas_call(functools.partial(gather_kernel, axis, count), out_shape=j...  26.1 us
    pallas_call x1, Pallas kernels, attend(): pl.pallas_call(functools.partial(attend_kernel, rows, dims), grid=(count...  25.7 us
    pallas_call x1, Pallas kernels, project_out(): pl.pallas_call(functools.partial(project_out_kernel, axis, count), out_sh...  13.2 us
    dot_general x3, matrix products, project(): jnp.einsum('nd,gdk->gnk', normed, parts, preferred_element_type=jnp.float32)  7.41 us
    unnamed x26, local copies, waits for them, and re-layouts  4.27 us

profile of v1, /device:TPU:12, one launch (start us, length us, event | category | flops | bytes accessed | tf_op | source)
XLA Modules:
  0.0 142.9 jit_solution(10381129389000177483)
XLA Ops:
  0.6 0.0 copy-start
  0.7 0.1 pad.6.clone
  0.7 1.6 %fusion.6 = f32[112]{0:T(128)S(1)} fusion(bf16[1,4096]{1,0:T(2,128)(2,1)} %param.16, bf16[96,4096]{1,0:T(8,128)(2,1)} %param.15, bf16[112]{0:T(256)(128)(2,1)S(1)} %pad.6.clone), kind=kLoop, calls=%fused_computation.9 | loop fusion | flops 3669904 | bytes 795296 | tf_op jit(solution)/shard_map/reduce_sum | solution.py:19
  2.4 0.0 copy-start.4
  2.4 0.0 copy-start.5
  2.4 0.0 copy-start.8
  2.4 0.0 copy-start.10
  2.4 3.5 %fusion.21 = bf16[4,112,128]{2,1,0:T(8,128)(2,1)S(1)} fusion(bf16[4,4096,128]{2,0,1:T(4,128)(2,1)} %bitcast.64, f32[4096]{0:T(1024)} %param.17, f32[112]{0:T(128)S(1)} %add_rsqrt_fusion, bf16[1,4096]{1,0:T(2,128)(2,1)} %param.16, bf16[96,4096]{1,0:T(8,128)(2,1)} %param.15, bf16[112]{0:T(256)(128)(2,1)S(1)} %pad.6.clone), kind=kOutput, calls=%fused_computation.16 | convolution fusion | flops 473948160 | bytes 5120672 | tf_op jit(solution)/shard_map/nd,gdk->gnk/dot_general | solution.py:27
  5.9 0.0 copy-start.6
  6.0 0.0 copy-done.4
  6.0 0.0 copy-done.5
  6.0 0.4 copy-done.8
  6.4 0.0 copy-done.10
  6.4 0.0 copy-start.9
  6.4 0.9 fusion.24
  7.3 0.0 copy-done.6
  7.3 0.0 copy-start.7
  7.3 0.7 copy.101
  7.9 26.1 %gather_rows.1.q_ref = bf16[8,112,512]{2,1,0:T(8,128)(2,1)} custom-call(bf16[112,512]{1,0:T(8,128)(2,1)} %bitcast.52), custom_call_target="tpu_custom_call" | custom-call | tf_op jit(solution)/shard_map/gather_rows/pallas_call | solution.py:62
  34.1 0.9 slice.25
  35.0 0.0 copy-done.9
  35.0 0.6 fusion.28
  35.6 0.0 copy-done.7
  35.6 0.1 broadcast_compare_fusion
  35.7 0.1 multiply_reduce_fusion
  35.9 0.1 fusion.38
  36.0 3.1 %fusion.18 = bf16[2,112,256]{2,1,0:T(8,128)(2,1)S(1)} fusion(bf16[2,4096,256]{2,0,1:T(2,128)(2,1)} %bitcast.66, f32[4096]{0:T(1024)S(1)} %copy-done.10, f32[112]{0:T(128)S(1)} %add_rsqrt_fusion, bf16[1,4096]{1,0:T(2,128)(2,1)S(1)} %copy-done.5, bf16[96,4096]{1,0:T(8,128)(2,1)S(1)} %copy-done.4, bf16[112]{0:T(256)(128)(2,1)S(1)} %pad.6.clone), kind=kOutput, calls=%fused_computation.15 | convolution fusion | flops 473948160 | bytes 5120672 | tf_op jit(solution)/shard_map/nd,gdk->gnk/dot_general | solution.py:27
  39.0 0.0 copy-start.1
  39.1 0.6 constant_dynamic-update-slice_fusion
  39.6 0.0 copy-done
  39.6 0.3 fusion.27
  40.0 0.2 fusion.33
  40.2 0.1 fusion.37
  40.3 0.1 copy.57
  40.3 0.1 copy.59
  40.5 0.1 copy.56
  40.5 0.1 copy.58
  40.7 0.1 pad.3.clone
  40.7 0.7 maximum_maximum_fusion.1.step
  41.4 0.7 slice_bitcast_fusion
  42.1 0.6 slice.30.fk_ref
  43.4 0.6 compare_select_fusion.bias_ref
  44.0 0.5 iota_add_fusion.1.own_ref
  44.5 0.0 copy-done.1
  44.5 0.0 copy-start.2
  44.5 1.6 %copy.100 = bf16[2048,2,256]{2,0,1:T(8,128)(2,1)} copy(bf16[2048,2,256]{2,1,0:T(2,128)(2,1)S(1)} %copy-done.1) | data formatting | bytes 4194304 | tf_op args[10]
  46.1 0.8 copy-done.2
  46.9 1.6 %copy.50 = bf16[2,2,2048,128]{3,2,1,0:T(8,128)(2,1)} copy(bf16[2,2,2048,128]{3,1,0,2:T(2,128)(2,1)S(1)} %bitcast.50) | data formatting | bytes 4194304 | tf_op jit(solution)/shard_map/transpose | solution.py:373
  48.5 25.7 %attend.1 = (bf16[8,96,1024]{2,1,0:T(8,128)(2,1)}, f32[8,96,128]{2,1,0:T(8,128)}) custom-call(bf16[8,112,512]{2,1,0:T(8,128)(2,1)} %gather_rows.1.q_ref, bf16[4,2048,128]{2,1,0:T(8,128)(2,1)} %bitcast.48, bf16[2,2048,256]{2,1,0:T(8,128)(2,1)} %bitcast.47, bf16[4,96,128]{2,1,0:T(8,128)(2,1)} %slice.30.fk_ref, bf16[2,96,256]{2,1,0:T(8,128)(2,1)} %get-tuple-element.33.fv_ref, ...), custom_call_target="tpu_custom_call" | custom-call | tf_op jit(solution)/shard_map/attend/pallas_call | solution.py:117
  74.2 51.1 %exchange.1.heads = bf16[112,512]{1,0:T(8,128)(2,1)} custom-call(f32[1,2]{1,0:T(1,128)} %bitcast.63, f32[1,256]{1,0:T(1,128)} %bitcast.62, bf16[8,96,1024]{2,1,0:T(8,128)(2,1)} %get-tuple-element.8.vals, f32[8,96,128]{2,1,0:T(8,128)} %get-tuple-element.9.stats, f32[8,4,384]{2,1,0:T(4,128)} %maximum_maximum_fusion.1.step), custom_call_target="tpu_custom_call" | custom-call | tf_op jit(solution)/shard_map/exchange/pallas_call | solution.py:232
  125.3 0.0 copy-start.3
  125.3 13.2 %project_out.1 = bf16[112,1024]{1,0:T(8,128)(2,1)} custom-call(bf16[112,512]{1,0:T(8,128)(2,1)} %exchange.1.heads, bf16[512,4096]{1,0:T(8,128)(2,1)} %bitcast.49), custom_call_target="tpu_custom_call" | custom-call | tf_op jit(solution)/shard_map/project_out/pallas_call | solution.py:305
  138.5 1.6 %slice.28 = bf16[96,1024]{1,0:T(8,128)(2,1)} slice(bf16[112,1024]{1,0:T(8,128)(2,1)} %project_out.1), slice={[0:96], [0:1024]} | slice | bytes 393216 | tf_op jit(solution)/shard_map/slice | solution.py:446
  140.2 1.3 slice.29
  141.5 0.7 copy.61
  142.2 0.0 copy-done.3
  142.2 0.7 copy.60
  (16 shorter events, 0.1 us)
Async XLA Ops:
  0.6 39.0 %copy-start = (bf16[8,128,2,256]{3,2,1,0:T(2,128)(2,1)S(1)}, bf16[8,128,2,256]{3,2,1,0:T(2,128)(2,1)}, u32[]{:S(2)}) copy-start(bf16[8,128,2,256]{3,2,1,0:T(2,128)(2,1)} %param.27) | copy-start | bytes 3145732
  2.4 3.6 %copy-start.4 = (bf16[96,4096]{1,0:T(8,128)(2,1)S(1)}, bf16[96,4096]{1,0:T(8,128)(2,1)}, u32[]{:S(2)}) copy-start(bf16[96,4096]{1,0:T(8,128)(2,1)} %param.15) | copy-start | bytes 2359300
  2.4 3.6 %copy-start.5 = (bf16[1,4096]{1,0:T(2,128)(2,1)S(1)}, bf16[1,4096]{1,0:T(2,128)(2,1)}, u32[]{:S(2)}) copy-start(bf16[1,4096]{1,0:T(2,128)(2,1)} %param.16) | copy-start | bytes 24580
  2.4 4.0 %copy-start.8 = (bf16[4096,2,2,128]{3,2,1,0:T(2,128)(2,1)S(1)}, bf16[4096,2,2,128]{3,2,1,0:T(2,128)(2,1)}, u32[]{:S(2)}) copy-start(bf16[4096,2,2,128]{3,2,1,0:T(2,128)(2,1)} %param.18) | copy-start | bytes 12582916
  2.4 4.0 %copy-start.10 = (f32[4096]{0:T(1024)S(1)}, f32[4096]{0:T(1024)}, u32[]{:S(2)}) copy-start(f32[4096]{0:T(1024)} %param.17) | copy-start | bytes 49156
  5.9 1.3 copy-start.6
  6.4 28.6 %copy-start.9 = (bf16[8,128,2,2,128]{4,3,2,1,0:T(2,128)(2,1)S(1)}, bf16[8,128,2,2,128]{4,3,2,1,0:T(2,128)(2,1)}, u32[]{:S(2)}) copy-start(bf16[8,128,2,2,128]{4,3,2,1,0:T(2,128)(2,1)} %param.26) | copy-start | bytes 3145732
  7.3 28.4 %copy-start.7 = (s32[8]{0:T(128)S(1)}, s32[8]{0:T(128)}, u32[]{:S(2)}) copy-start(s32[8]{0:T(128)} %param.29) | copy-start | bytes 100
  39.0 5.5 %copy-start.1 = (bf16[2048,2,256]{2,1,0:T(2,128)(2,1)S(1)}, bf16[2048,2,256]{2,1,0:T(2,128)(2,1)}, u32[]{:S(2)}) copy-start(bf16[2048,2,256]{2,1,0:T(2,128)(2,1)} %param.25) | copy-start | bytes 6291460
  44.5 2.3 %copy-start.2 = (bf16[2048,2,2,128]{3,2,1,0:T(2,128)(2,1)S(1)}, bf16[2048,2,2,128]{3,2,1,0:T(2,128)(2,1)}, u32[]{:S(2)}) copy-start(bf16[2048,2,2,128]{3,2,1,0:T(2,128)(2,1)} %param.24) | copy-start | bytes 6291460
  125.3 16.9 %copy-start.3 = (bf16[4,96,128]{2,1,0:T(8,128)(2,1)S(1)}, bf16[4,96,128]{2,1,0:T(8,128)(2,1)}, u32[]{:S(2)}) copy-start(bf16[4,96,128]{2,1,0:T(8,128)(2,1)} %slice.30.fk_ref) | copy-start | bytes 294916

commit v2 on v1

--- a/solution.py
+++ b/solution.py
@@ -39,34 +39,102 @@
     return me
 
 
-def gather_kernel(axis, count, own, everyone, send_sem, recv_sem):
-    me = meet(axis, count)
-    copies = []
-    for step in range(1, count):
-        copy = pltpu.make_async_remote_copy(
+def grid_of(count):
+    across = max(c for c in range(1, count + 1) if count % c == 0 and c * c <= max(count // 2, 1))
+    return across, count // across
+
+
+def gather_kernel(axis, across, along, own, everyone, z_send, z_recv, y_send, y_recv):
+    me = meet(axis, across * along)
+    z, y = me // across, lax.rem(me, across)
+
+    def hop(way, far):
+        step = 1 - 2 * way
+        unit = (z - step * far) * across + y
+        return pltpu.make_async_remote_copy(
+            src_ref=own if far == 0 else everyone.at[unit],
+            dst_ref=everyone.at[unit],
+            send_sem=z_send.at[way, far],
+            recv_sem=z_recv.at[way, far],
+            device_id={axis: (z + step) * across + y},
+            device_id_type=MESH,
+        )
+
+    def arrival(way, far):
+        step = 1 - 2 * way
+        unit = (z - step * far) * across + y
+        return pltpu.make_async_remote_copy(
             src_ref=own,
-            dst_ref=everyone.at[me],
-            send_sem=send_sem.at[step],
-            recv_sem=recv_sem.at[step],
-            device_id={axis: lax.rem(me + step, count)},
+            dst_ref=everyone.at[unit],
+            send_sem=z_send.at[way, far - 1],
+            recv_sem=z_recv.at[way, far - 1],
+            device_id={axis: (z - step) * across + y},
             device_id_type=MESH,
         )
-        copy.start()
-        copies.append(copy)
+
+    def relay(turn, place, source):
+        return pltpu.make_async_remote_copy(
+            src_ref=source,
+            dst_ref=everyone.at[place * across + y],
+            send_sem=y_send.at[turn, place],
+            recv_sem=y_recv.at[turn, place],
+            device_id={axis: z * across + lax.rem(y + turn, across)},
+            device_id_type=MESH,
+        )
+
+    def can_go(way):
+        return z < along - 1 if way == 0 else z > 0
+
+    def has(way, far):
+        return z - far >= 0 if way == 0 else z + far < along
+
+    for way in range(2):
+        pl.when(can_go(way))(lambda way=way: hop(way, 0).start())
+    for turn in range(1, across):
+        relay(turn, z, own).start()
     everyone[me] = own[...]
-    for copy in copies:
-        copy.wait()
+    for far in range(1, along):
+        for way in range(2):
+
+            @pl.when(has(way, far))
+            def _():
+                arrival(way, far).wait_recv()
+                if far < along - 1:
+                    pl.when(can_go(way))(lambda: hop(way, far).start())
+                place = z - far if way == 0 else z + far
+                for turn in range(1, across):
+                    relay(turn, place, everyone.at[place * across + y]).start()
+
+    for turn in range(1, across):
+        came = lax.rem(y + across - turn, across)
+        for place in range(along):
+            pltpu.make_async_remote_copy(
+                src_ref=own,
+                dst_ref=everyone.at[place * across + came],
+                send_sem=y_send.at[turn, place],
+                recv_sem=y_recv.at[turn, place],
+                device_id={axis: z * across + came},
+                device_id_type=MESH,
+            ).wait_recv()
+            relay(turn, place, own).wait_send()
+    for way in range(2):
+        for far in range(along - 1):
+            live = can_go(way) if far == 0 else jnp.logical_and(can_go(way), has(way, far))
+            pl.when(live)(lambda way=way, far=far: hop(way, far).wait_send())
 
 
 def gather_rows(own, axis, count, collective):
+    across, along = grid_of(count)
     return pl.pallas_call(
-        functools.partial(gather_kernel, axis, count),
+        functools.partial(gather_kernel, axis, across, along),
         out_shape=jax.ShapeDtypeStruct((count,) + own.shape, own.dtype),
         in_specs=[pl.BlockSpec(memory_space=pltpu.VMEM)],
         out_specs=pl.BlockSpec(memory_space=pltpu.VMEM),
         scratch_shapes=[
-            pltpu.SemaphoreType.DMA((count,)),
-            pltpu.SemaphoreType.DMA((count,)),
+            pltpu.SemaphoreType.DMA((2, along)),
+            pltpu.SemaphoreType.DMA((2, along)),
+            pltpu.SemaphoreType.DMA((across, along)),
+            pltpu.SemaphoreType.DMA((across, along)),
         ],
         compiler_params=pltpu.CompilerParams(collective_id=collective, has_side_effects=True),
         name="gather_rows",
@@ -93,19 +161,18 @@
     total = jnp.sum(old_w, axis=1, keepdims=True) + jnp.sum(new_w, axis=1, keepdims=True)
     summed = jnp.dot(old_w.astype(jnp.bfloat16), v_ref[0], preferred_element_type=jnp.float32)
     summed += jnp.dot(new_w.astype(jnp.bfloat16), fv_ref[0], preferred_element_type=jnp.float32)
-    o_ref[...] = summed.astype(jnp.bfloat16).reshape(o_ref.shape)
-    parts = pl.num_programs(1)
-    lane = lax.broadcasted_iota(jnp.int32, (owners * rows, s_ref.shape[-1]), 1)
-    put = jnp.where(lane == part, top * scale, jnp.where(lane == parts + part, total, 0.0))
-    put = put.reshape(s_ref.shape)
+    o_ref[...] = (summed / total).astype(jnp.bfloat16).reshape(o_ref.shape)
+    lane = lax.broadcasted_iota(jnp.int32, (owners * rows, 128), 1)
+    put = jnp.where(lane == part, top * scale + jnp.log(total), 0.0)
+    put = jnp.transpose(put)[: s_ref.shape[1]]
 
     @pl.when(part == 0)
     def _():
-        s_ref[...] = put
+        s_ref[0] = put
 
     @pl.when(part != 0)
     def _():
-        s_ref[...] += put
+        s_ref[0] += put
 
 
 def attend(q_all, keys, values, fresh_k, fresh_v, bias, fresh_place, rows):
@@ -113,7 +180,7 @@
     parts, cached, dims = keys.shape
     maps = parts // values.shape[0]
     wide = values.shape[-1]
-    owners = math.gcd(count, 2)
+    owners = math.gcd(count, 4)
     return pl.pallas_call(
         functools.partial(attend_kernel, rows, dims),
         grid=(count // owners, parts),
@@ -128,11 +195,11 @@
         ],
         out_specs=[
             pl.BlockSpec((owners, rows, wide), lambda i, p: (i, 0, p)),
-            pl.BlockSpec((owners, rows, 128), lambda i, p: (i, 0, 0)),
+            pl.BlockSpec((1, 8, owners * rows), lambda i, p: (i, 0, 0)),
         ],
         out_shape=[
             jax.ShapeDtypeStruct((count, rows, parts * wide), jnp.bfloat16),
-            jax.ShapeDtypeStruct((count, rows, 128), jnp.float32),
+            jax.ShapeDtypeStruct((count // owners, 8, owners * rows), jnp.float32),
         ],
         compiler_params=pltpu.CompilerParams(
             dimension_semantics=("arbitrary", "arbitrary"), vmem_limit_bytes=56 * 1024 * 1024
@@ -141,8 +208,7 @@
     )(q_all, keys, values, fresh_k, fresh_v, bias, fresh_place)
 
 
-def mix_maps(first, second, ratio, gain):
-    mixed = first - ratio * second
+def shape_head(mixed, gain):
     inv_rms = lax.rsqrt(jnp.mean(mixed * mixed, axis=-1, keepdims=True) + EPS)
     return (mixed * inv_rms * gain * OUT_SCALE).astype(jnp.bfloat16)
 
@@ -157,54 +223,164 @@
 
 
 def exchange_kernel(
-    axis, count, parts, maps, wide, ratio, gain, vals, stats, step, out, all_v, all_s, all_t, send_sem, recv_sem
+    axis,
+    across,
+    along,
+    parts,
+    maps,
+    wide,
+    ratio,
+    gain,
+    vals,
+    stats,
+    step,
+    out,
+    all_s,
+    all_t,
+    mine,
+    total,
+    y_in,
+    z_in,
+    z_out,
+    m_send,
+    m_recv,
+    y_send,
+    y_recv,
+    z_send,
+    z_recv,
 ):
+    count = across * along
     me = meet(axis, count)
+    z, y = me // across, lax.rem(me, across)
     copies = []
     for turn in range(1, count):
         other = lax.rem(me + turn, count)
-        for slot, (mine, theirs) in enumerate(((stats, all_s), (step, all_t), (vals, all_v))):
+        for slot, (own, theirs) in enumerate(((stats, all_s.at[me]), (step.at[other], all_t.at[me]))):
             copy = pltpu.make_async_remote_copy(
-                src_ref=mine.at[other],
-                dst_ref=theirs.at[me],
-                send_sem=send_sem.at[turn, slot],
-                recv_sem=recv_sem.at[turn, slot],
+                src_ref=own,
+                dst_ref=theirs,
+                send_sem=m_send.at[turn, slot],
+                recv_sem=m_recv.at[turn, slot],
                 device_id={axis: other},
                 device_id_type=MESH,
             )
             copy.start()
             copies.append(copy)
-    all_v[me] = vals[me]
-    all_s[me] = stats[me]
+    all_s[me] = stats[...]
     all_t[me] = step[me]
     for copy in copies:
         copy.wait()
     rows = vals.shape[1]
     steps = step.shape[1] // parts
-    out[...] = jnp.zeros_like(out)
-    tall = math.gcd(rows, 32)
-
-    def chunk(index, carry):
-        at = pl.ds(pl.multiple_of(index * tall, tall), tall)
-        for head in range(parts // maps):
-            maps_out = []
-            for part in range(head * maps, head * maps + maps):
-                cut = slice(part * wide, part * wide + wide)
-                maps_out.append(
-                    blend(
-                        [all_v[g, at, cut].astype(jnp.float32) for g in range(count)],
-                        [all_s[g, at, part : part + 1] for g in range(count)],
-                        [all_s[g, at, parts + part : parts + part + 1] for g in range(count)],
+    heads = parts // maps
+    blocks, lines, length = stats.shape
+    owners = length // rows
+    which = lax.broadcasted_iota(jnp.int32, (lines, length), 0)
+    sign = jnp.ones((lines, length), jnp.float32)
+    for head in range(heads):
+        sign = jnp.where(which == head * maps + 1, -ratio[0, head], sign)
+    for block in range(blocks):
+        best = functools.reduce(jnp.maximum, [all_s[g, block] for g in range(count)])
+        norm = functools.reduce(jnp.add, [jnp.exp(all_s[g, block] - best) for g in range(count)])
+        share = jnp.exp(stats[block] - best) / norm * sign
+        share = jnp.concatenate([share, jnp.zeros((128 - lines, length), jnp.float32)], axis=0)
+        column = jnp.transpose(share)
+        for owner in range(owners):
+            to = block * owners + owner
+            c = column[owner * rows : owner * rows + rows]
+            for head in range(heads):
+                acc = None
+                for part in range(head * maps, head * maps + maps):
+                    term = c[:, part : part + 1] * vals[to, :, part * wide : part * wide + wide].astype(
+                        jnp.float32
                     )
-                )
-            out[at, head * wide : head * wide + wide] = mix_maps(
-                maps_out[0], maps_out[1], ratio[0, head], gain[...]
+                    acc = term if acc is None else acc + term
+                mine[to, :, head * wide : head * wide + wide] = acc.astype(jnp.bfloat16)
+    order = sorted(range(along), key=lambda p: (-abs(2 * p - along + 1), -p))
+
+    def over_y(turn, place):
+        other = lax.rem(y + turn, across)
+        return pltpu.make_async_remote_copy(
+            src_ref=mine.at[place * across + other],
+            dst_ref=y_in.at[turn, place],
+            send_sem=y_send.at[turn, place],
+            recv_sem=y_recv.at[turn, place],
+            device_id={axis: z * across + other},
+            device_id_type=MESH,
+        )
+
+    def over_z(way, place):
+        return pltpu.make_async_remote_copy(
+            src_ref=z_out.at[place],
+            dst_ref=z_in.at[way, place],
+            send_sem=z_send.at[way, place],
+            recv_sem=z_recv.at[way, place],
+            device_id={axis: (z + 1 - 2 * way) * across + y},
+            device_id_type=MESH,
+        )
+
+    def from_z(way, place):
+        return pltpu.make_async_remote_copy(
+            src_ref=z_out.at[place],
+            dst_ref=z_in.at[way, place],
+            send_sem=z_send.at[way, place],
+            recv_sem=z_recv.at[way, place],
+            device_id={axis: (z - 1 + 2 * way) * across + y},
+            device_id_type=MESH,
+        )
+
+    for place in order:
+        for turn in range(1, across):
+            over_y(turn, place).start()
+    for place in order:
+        for turn in range(1, across):
+            over_y(turn, place).wait_recv()
+        both = mine[place * across + y].astype(jnp.float32)
+        for turn in range(1, across):
+            both = both + y_in[turn, place].astype(jnp.float32)
+        total[...] = both
+
+        @pl.when(z == place)
+        def _():
+            total_own = both
+            mixed_ref = z_out.at[place]
+            mixed_ref[...] = total_own.astype(jnp.bfloat16)
+
+        for way in range(2):
+            moves = z < place if way == 0 else z > place
+            behind = z > 0 if way == 0 else z < along - 1
+
+            @pl.when(moves)
+            def _():
+                @pl.when(behind)
+                def _():
+                    from_z(way, place).wait_recv()
+                    total[...] += z_in[way, place].astype(jnp.float32)
+
+                z_out[place] = total[...].astype(jnp.bfloat16)
+                over_z(way, place).start()
+
+    for place in range(along):
+
+        @pl.when(z == place)
+        def _():
+            total[...] = z_out[place].astype(jnp.float32)
+            for way in range(2):
+                if (way == 0 and place > 0) or (way == 1 and place < along - 1):
+                    from_z(way, place).wait_recv()
+                    total[...] += z_in[way, place].astype(jnp.float32)
+
+        for way in range(2):
+            pl.when(z < place if way == 0 else z > place)(
+                lambda way=way, place=place: over_z(way, place).wait_send()
             )
-        return carry
-
-    lax.fori_loop(0, rows // tall, chunk, 0)
+        for turn in range(1, across):
+            over_y(turn, place).wait_send()
+    for head in range(heads):
+        cut = slice(head * wide, head * wide + wide)
+        out[:rows, cut] = shape_head(total[:, cut], gain[...])
     low = out.shape[0] - rows
-    for head in range(parts // maps):
+    for head in range(heads):
         lines = []
         for seq in range(steps):
             maps_out = []
@@ -217,7 +393,7 @@
                         [v[:, wide + 1 : wide + 2] for v in line],
                     )
                 )
-            lines.append(mix_maps(maps_out[0], maps_out[1], ratio[0, head], gain[...]).astype(jnp.float32))
+            lines.append(shape_head(maps_out[0] - ratio[0, head] * maps_out[1], gain[...]).astype(jnp.float32))
         place = lax.broadcasted_iota(jnp.int32, (low, wide), 0)
         block = jnp.zeros((low, wide), jnp.float32)
         for seq in range(steps):
@@ -226,20 +402,31 @@
 
 
 def exchange(values, stats, step, ratio, gain, axis, count, maps, padded, collective):
+    across, along = grid_of(count)
     parts = values.shape[-1] // gain.shape[-1]
     wide = gain.shape[-1]
+    rows = values.shape[1]
+    flat = parts // maps * wide
     vmem = pl.BlockSpec(memory_space=pltpu.VMEM)
     return pl.pallas_call(
-        functools.partial(exchange_kernel, axis, count, parts, maps, wide),
-        out_shape=jax.ShapeDtypeStruct((padded, parts // maps * wide), jnp.bfloat16),
+        functools.partial(exchange_kernel, axis, across, along, parts, maps, wide),
+        out_shape=jax.ShapeDtypeStruct((padded, flat), jnp.bfloat16),
         in_specs=[pl.BlockSpec(memory_space=pltpu.SMEM), vmem, vmem, vmem, vmem],
         out_specs=vmem,
         scratch_shapes=[
-            pltpu.VMEM(values.shape, values.dtype),
-            pltpu.VMEM(stats.shape, stats.dtype),
+            pltpu.VMEM((count,) + stats.shape, stats.dtype),
             pltpu.VMEM(step.shape, step.dtype),
-            pltpu.SemaphoreType.DMA((count, 3)),
-            pltpu.SemaphoreType.DMA((count, 3)),
+            pltpu.VMEM((count, rows, flat), jnp.bfloat16),
+            pltpu.VMEM((rows, flat), jnp.float32),
+            pltpu.VMEM((across, along, rows, flat), jnp.bfloat16),
+            pltpu.VMEM((2, along, rows, flat), jnp.bfloat16),
+            pltpu.VMEM((along, rows, flat), jnp.bfloat16),
+            pltpu.SemaphoreType.DMA((count, 2)),
+            pltpu.SemaphoreType.DMA((count, 2)),
+            pltpu.SemaphoreType.DMA((across, along)),
+            pltpu.SemaphoreType.DMA((across, along)),
+            pltpu.SemaphoreType.DMA((2, along)),
+            pltpu.SemaphoreType.DMA((2, along)),
         ],
         compiler_params=pltpu.CompilerParams(
             collective_id=collective, has_side_effects=True, vmem_limit_bytes=56 * 1024 * 1024

time: 143 us -> 116 us (0.81)
  the two profiles are of different devices: /device:TPU:12 before, /device:TPU:0 now
where the time goes in v2:
time: 116 us
  Pallas kernels  88.9 us (77%)
  local copies, waits for them, and re-layouts  12.8 us (11%)
  matrix products  8.34 us (7%)
  other arithmetic  4.02 us (3%)
  between operations  1.57 us (1%)
    pallas_call x1, Pallas kernels, exchange(): pl.pallas_call(functools.partial(exchange_kernel, axis, across, along, pa...  31.2 us
    pallas_call x1, Pallas kernels, gather_rows(): pl.pallas_call(functools.partial(gather_kernel, axis, across, along), out...  22.5 us
    pallas_call x1, Pallas kernels, attend(): pl.pallas_call(functools.partial(attend_kernel, rows, dims), grid=(count...  22.1 us
    pallas_call x1, Pallas kernels, project_out(): pl.pallas_call(functools.partial(project_out_kernel, axis, count), out_sh...  13.2 us
    dot_general x3, matrix products, project(): jnp.einsum('nd,gdk->gnk', normed, parts, preferred_element_type=jnp.float32)  7.4 us
    unnamed x26, local copies, waits for them, and re-layouts  4.28 us

profile of v2, /device:TPU:0, one launch (start us, length us, event | category | flops | bytes accessed | tf_op | source)
XLA Modules:
  0.0 115.7 jit_solution(18305672533048124712)
XLA Ops:
  0.6 0.0 copy-start
  0.7 0.1 pad.6.clone
  0.7 1.6 %fusion.6 = f32[112]{0:T(128)S(1)} fusion(bf16[1,4096]{1,0:T(2,128)(2,1)} %param.16, bf16[96,4096]{1,0:T(8,128)(2,1)} %param.15, bf16[112]{0:T(256)(128)(2,1)S(1)} %pad.6.clone), kind=kLoop, calls=%fused_computation.9 | loop fusion | flops 3669904 | bytes 795296 | tf_op jit(solution)/shard_map/reduce_sum | solution.py:19
  2.4 0.0 copy-start.4
  2.4 0.0 copy-start.5
  2.4 0.0 copy-start.8
  2.4 0.0 copy-start.10
  2.4 3.5 %fusion.21 = bf16[4,112,128]{2,1,0:T(8,128)(2,1)S(1)} fusion(bf16[4,4096,128]{2,0,1:T(4,128)(2,1)} %bitcast.64, f32[4096]{0:T(1024)} %param.17, f32[112]{0:T(128)S(1)} %add_rsqrt_fusion, bf16[1,4096]{1,0:T(2,128)(2,1)} %param.16, bf16[96,4096]{1,0:T(8,128)(2,1)} %param.15, bf16[112]{0:T(256)(128)(2,1)S(1)} %pad.6.clone), kind=kOutput, calls=%fused_computation.16 | convolution fusion | flops 473948160 | bytes 5120672 | tf_op jit(solution)/shard_map/nd,gdk->gnk/dot_general | solution.py:27
  5.9 0.0 copy-start.6
  5.9 0.0 copy-done.4
  6.0 0.0 copy-done.5
  6.0 0.4 copy-done.8
  6.4 0.0 copy-done.10
  6.4 0.0 copy-start.9
  6.4 0.9 fusion.24
  7.3 0.0 copy-done.6
  7.3 0.0 copy-start.7
  7.3 0.7 copy.101
  7.9 22.5 %gather_rows.1.q_ref = bf16[8,112,512]{2,1,0:T(8,128)(2,1)} custom-call(bf16[112,512]{1,0:T(8,128)(2,1)} %bitcast.52), custom_call_target="tpu_custom_call" | custom-call | tf_op jit(solution)/shard_map/gather_rows/pallas_call | solution.py:128
  30.4 0.9 slice.25
  31.3 0.0 copy-done.9
  31.3 0.6 fusion.28
  31.9 0.0 copy-done.7
  32.0 0.1 broadcast_compare_fusion
  32.0 0.1 multiply_reduce_fusion
  32.2 0.1 fusion.38
  32.3 3.1 %fusion.18 = bf16[2,112,256]{2,1,0:T(8,128)(2,1)S(1)} fusion(bf16[2,4096,256]{2,0,1:T(2,128)(2,1)} %bitcast.66, f32[4096]{0:T(1024)S(1)} %copy-done.10, f32[112]{0:T(128)S(1)} %add_rsqrt_fusion, bf16[1,4096]{1,0:T(2,128)(2,1)S(1)} %copy-done.5, bf16[96,4096]{1,0:T(8,128)(2,1)S(1)} %copy-done.4, bf16[112]{0:T(256)(128)(2,1)S(1)} %pad.6.clone), kind=kOutput, calls=%fused_computation.15 | convolution fusion | flops 473948160 | bytes 5120672 | tf_op jit(solution)/shard_map/nd,gdk->gnk/dot_general | solution.py:27
  35.4 0.0 copy-start.1
  35.4 0.6 constant_dynamic-update-slice_fusion
  36.0 0.0 copy-done
  36.0 0.3 fusion.27
  36.3 0.2 fusion.33
  36.5 0.1 fusion.37
  36.6 0.1 copy.57
  36.7 0.1 copy.59
  36.8 0.1 copy.56
  36.9 0.1 copy.58
  37.0 0.1 pad.3.clone
  37.1 0.7 maximum_maximum_fusion.1.step
  37.8 0.7 slice_bitcast_fusion
  38.4 0.6 slice.30.fk_ref
  39.7 0.6 compare_select_fusion.bias_ref
  40.3 0.5 iota_add_fusion.1.own_ref
  40.8 0.0 copy-done.1
  40.8 0.0 copy-start.2
  40.9 1.6 %copy.100 = bf16[2048,2,256]{2,0,1:T(8,128)(2,1)} copy(bf16[2048,2,256]{2,1,0:T(2,128)(2,1)S(1)} %copy-done.1) | data formatting | bytes 4194304 | tf_op args[10]
  42.4 0.8 copy-done.2
  43.2 1.6 %copy.50 = bf16[2,2,2048,128]{3,2,1,0:T(8,128)(2,1)} copy(bf16[2,2,2048,128]{3,1,0,2:T(2,128)(2,1)S(1)} %bitcast.50) | data formatting | bytes 4194304 | tf_op jit(solution)/shard_map/transpose | solution.py:560
  44.8 22.1 %attend.1 = (bf16[8,96,1024]{2,1,0:T(8,128)(2,1)}, f32[2,8,384]{2,1,0:T(8,128)}) custom-call(bf16[8,112,512]{2,1,0:T(8,128)(2,1)} %gather_rows.1.q_ref, bf16[4,2048,128]{2,1,0:T(8,128)(2,1)} %bitcast.48, bf16[2,2048,256]{2,1,0:T(8,128)(2,1)} %bitcast.47, bf16[4,96,128]{2,1,0:T(8,128)(2,1)} %slice.30.fk_ref, bf16[2,96,256]{2,1,0:T(8,128)(2,1)} %get-tuple-element.33.fv_ref, ...), custom_call_target="tpu_custom_call" | custom-call | tf_op jit(solution)/shard_map/attend/pallas_call | solution.py:184
  66.9 31.2 %exchange.1.heads = bf16[112,512]{1,0:T(8,128)(2,1)} custom-call(f32[1,2]{1,0:T(1,128)} %bitcast.63, f32[1,256]{1,0:T(1,128)} %bitcast.62, bf16[8,96,1024]{2,1,0:T(8,128)(2,1)} %get-tuple-element.8.vals, f32[2,8,384]{2,1,0:T(8,128)} %get-tuple-element.9.stats, f32[8,4,384]{2,1,0:T(4,128)} %maximum_maximum_fusion.1.step), custom_call_target="tpu_custom_call" | custom-call | tf_op jit(solution)/shard_map/exchange/pallas_call | solution.py:411
  98.1 0.0 copy-start.3
  98.1 13.2 %project_out.1 = bf16[112,1024]{1,0:T(8,128)(2,1)} custom-call(bf16[112,512]{1,0:T(8,128)(2,1)} %exchange.1.heads, bf16[512,4096]{1,0:T(8,128)(2,1)} %bitcast.49), custom_call_target="tpu_custom_call" | custom-call | tf_op jit(solution)/shard_map/project_out/pallas_call | solution.py:492
  111.3 1.6 %slice.28 = bf16[96,1024]{1,0:T(8,128)(2,1)} slice(bf16[112,1024]{1,0:T(8,128)(2,1)} %project_out.1), slice={[0:96], [0:1024]} | slice | bytes 393216 | tf_op jit(solution)/shard_map/slice | solution.py:633
  112.9 1.3 %slice.29 = bf16[1,1024]{1,0:T(2,128)(2,1)} slice(bf16[112,1024]{1,0:T(8,128)(2,1)} %project_out.1), slice={[96:97], [0:1024]} | slice | bytes 4096 | tf_op jit(solution)/shard_map/slice | solution.py:633
  114.2 0.7 copy.61
  115.0 0.0 copy-done.3
  115.0 0.7 copy.60
  (16 shorter events, 0.1 us)
Async XLA Ops:
  0.6 35.3 %copy-start = (bf16[8,128,2,256]{3,2,1,0:T(2,128)(2,1)S(1)}, bf16[8,128,2,256]{3,2,1,0:T(2,128)(2,1)}, u32[]{:S(2)}) copy-start(bf16[8,128,2,256]{3,2,1,0:T(2,128)(2,1)} %param.27) | copy-start | bytes 3145732
  2.4 3.6 %copy-start.4 = (bf16[96,4096]{1,0:T(8,128)(2,1)S(1)}, bf16[96,4096]{1,0:T(8,128)(2,1)}, u32[]{:S(2)}) copy-start(bf16[96,4096]{1,0:T(8,128)(2,1)} %param.15) | copy-start | bytes 2359300
  2.4 3.6 %copy-start.5 = (bf16[1,4096]{1,0:T(2,128)(2,1)S(1)}, bf16[1,4096]{1,0:T(2,128)(2,1)}, u32[]{:S(2)}) copy-start(bf16[1,4096]{1,0:T(2,128)(2,1)} %param.16) | copy-start | bytes 24580
  2.4 4.0 %copy-start.8 = (bf16[4096,2,2,128]{3,2,1,0:T(2,128)(2,1)S(1)}, bf16[4096,2,2,128]{3,2,1,0:T(2,128)(2,1)}, u32[]{:S(2)}) copy-start(bf16[4096,2,2,128]{3,2,1,0:T(2,128)(2,1)} %param.18) | copy-start | bytes 12582916
  2.4 4.0 %copy-start.10 = (f32[4096]{0:T(1024)S(1)}, f32[4096]{0:T(1024)}, u32[]{:S(2)}) copy-start(f32[4096]{0:T(1024)} %param.17) | copy-start | bytes 49156
  5.9 1.4 %copy-start.6 = (bf16[4,1,128]{2,0,1:T(4,128)(2,1)}, bf16[4,1,128]{2,0,1:T(4,128)(2,1)S(1)}, u32[]{:S(2)}) copy-start(bf16[4,1,128]{2,0,1:T(4,128)(2,1)S(1)} %copy.68) | copy-start | bytes 3076
  6.4 24.9 %copy-start.9 = (bf16[8,128,2,2,128]{4,3,2,1,0:T(2,128)(2,1)S(1)}, bf16[8,128,2,2,128]{4,3,2,1,0:T(2,128)(2,1)}, u32[]{:S(2)}) copy-start(bf16[8,128,2,2,128]{4,3,2,1,0:T(2,128)(2,1)} %param.26) | copy-start | bytes 3145732
  7.3 24.7 %copy-start.7 = (s32[8]{0:T(128)S(1)}, s32[8]{0:T(128)}, u32[]{:S(2)}) copy-start(s32[8]{0:T(128)} %param.29) | copy-start | bytes 100
  35.4 5.5 %copy-start.1 = (bf16[2048,2,256]{2,1,0:T(2,128)(2,1)S(1)}, bf16[2048,2,256]{2,1,0:T(2,128)(2,1)}, u32[]{:S(2)}) copy-start(bf16[2048,2,256]{2,1,0:T(2,128)(2,1)} %param.25) | copy-start | bytes 6291460
  40.8 2.3 %copy-start.2 = (bf16[2048,2,2,128]{3,2,1,0:T(2,128)(2,1)S(1)}, bf16[2048,2,2,128]{3,2,1,0:T(2,128)(2,1)}, u32[]{:S(2)}) copy-start(bf16[2048,2,2,128]{3,2,1,0:T(2,128)(2,1)} %param.24) | copy-start | bytes 6291460
  98.1 16.9 %copy-start.3 = (bf16[4,96,128]{2,1,0:T(8,128)(2,1)S(1)}, bf16[4,96,128]{2,1,0:T(8,128)(2,1)}, u32[]{:S(2)}) copy-start(bf16[4,96,128]{2,1,0:T(8,128)(2,1)} %slice.30.fk_ref) | copy-start | bytes 294916

commit v3 on v2

--- a/solution.py
+++ b/solution.py
@@ -146,24 +146,28 @@
     owners = q_ref.shape[0]
     scale = dims ** (-0.5)
     fold = scale * math.log2(math.e)
-    q = q_ref[:, :rows, :].reshape(owners * rows, dims)
-    contract = (((1,), (1,)), ((), ()))
-    old = lax.dot_general(q, k_ref[0], contract, preferred_element_type=jnp.float32)
-    old = old + bias_ref[...]
-    new = lax.dot_general(q, fk_ref[0], contract, preferred_element_type=jnp.float32)
-    place = pl.program_id(0) * owners * rows + lax.broadcasted_iota(jnp.int32, new.shape, 0)
-    new = jnp.where(own_ref[...] <= place, new, HIDDEN)
-    top = jnp.maximum(
-        jnp.max(old, axis=1, keepdims=True), jnp.max(new, axis=1, keepdims=True)
-    )
-    old_w = jnp.exp2((old - top) * fold)
-    new_w = jnp.exp2((new - top) * fold)
-    total = jnp.sum(old_w, axis=1, keepdims=True) + jnp.sum(new_w, axis=1, keepdims=True)
-    summed = jnp.dot(old_w.astype(jnp.bfloat16), v_ref[0], preferred_element_type=jnp.float32)
-    summed += jnp.dot(new_w.astype(jnp.bfloat16), fv_ref[0], preferred_element_type=jnp.float32)
-    o_ref[...] = (summed / total).astype(jnp.bfloat16).reshape(o_ref.shape)
+    some = math.gcd(owners, 2)
+    logs = []
+    for at in range(0, owners, some):
+        q = q_ref[at : at + some, :rows, :].reshape(some * rows, dims)
+        contract = (((1,), (1,)), ((), ()))
+        old = lax.dot_general(q, k_ref[0], contract, preferred_element_type=jnp.float32)
+        old = old + bias_ref[...]
+        new = lax.dot_general(q, fk_ref[0], contract, preferred_element_type=jnp.float32)
+        place = (pl.program_id(0) * owners + at) * rows + lax.broadcasted_iota(jnp.int32, new.shape, 0)
+        new = jnp.where(own_ref[...] <= place, new, HIDDEN)
+        top = jnp.maximum(
+            jnp.max(old, axis=1, keepdims=True), jnp.max(new, axis=1, keepdims=True)
+        )
+        old_w = jnp.exp2((old - top) * fold)
+        new_w = jnp.exp2((new - top) * fold)
+        total = jnp.sum(old_w, axis=1, keepdims=True) + jnp.sum(new_w, axis=1, keepdims=True)
+        summed = jnp.dot(old_w.astype(jnp.bfloat16), v_ref[0], preferred_element_type=jnp.float32)
+        summed += jnp.dot(new_w.astype(jnp.bfloat16), fv_ref[0], preferred_element_type=jnp.float32)
+        o_ref[at : at + some] = (summed / total).astype(jnp.bfloat16).reshape(some, rows, -1)
+        logs.append(top * scale + jnp.log(total))
     lane = lax.broadcasted_iota(jnp.int32, (owners * rows, 128), 1)
-    put = jnp.where(lane == part, top * scale + jnp.log(total), 0.0)
+    put = jnp.where(lane == part, jnp.concatenate(logs, axis=0), 0.0)
     put = jnp.transpose(put)[: s_ref.shape[1]]
 
     @pl.when(part == 0)

time: 116 us -> 112 us (0.966)
  Pallas kernels: 88.9 us -> 85 us
    pallas_call x1, Pallas kernels: 22.1 us -> 18.1 us  [attend(): pl.pallas_call(functools.partial(attend_kernel, rows, dims), grid=(count...]
where the time goes in v3:
time: 112 us
  Pallas kernels  85 us (76%)
  local copies, waits for them, and re-layouts  12.8 us (11%)
  matrix products  8.34 us (7%)
  other arithmetic  4.02 us (4%)
  between operations  1.57 us (1%)
    pallas_call x1, Pallas kernels, exchange(): pl.pallas_call(functools.partial(exchange_kernel, axis, across, along, pa...  31.2 us
    pallas_call x1, Pallas kernels, gather_rows(): pl.pallas_call(functools.partial(gather_kernel, axis, across, along), out...  22.5 us
    pallas_call x1, Pallas kernels, attend(): pl.pallas_call(functools.partial(attend_kernel, rows, dims), grid=(count...  18.1 us
    pallas_call x1, Pallas kernels, project_out(): pl.pallas_call(functools.partial(project_out_kernel, axis, count), out_sh...  13.2 us
    dot_general x3, matrix products, project(): jnp.einsum('nd,gdk->gnk', normed, parts, preferred_element_type=jnp.float32)  7.4 us
    unnamed x26, local copies, waits for them, and re-layouts  4.28 us

profile of v3, /device:TPU:0, one launch (start us, length us, event | category | flops | bytes accessed | tf_op | source)
XLA Modules:
  0.0 111.7 jit_solution(9115524793998257467)
XLA Ops:
  0.6 0.0 copy-start
  0.7 0.1 pad.6.clone
  0.7 1.6 %fusion.6 = f32[112]{0:T(128)S(1)} fusion(bf16[1,4096]{1,0:T(2,128)(2,1)} %param.16, bf16[96,4096]{1,0:T(8,128)(2,1)} %param.15, bf16[112]{0:T(256)(128)(2,1)S(1)} %pad.6.clone), kind=kLoop, calls=%fused_computation.9 | loop fusion | flops 3669904 | bytes 795296 | tf_op jit(solution)/shard_map/reduce_sum | solution.py:19
  2.4 0.0 copy-start.4
  2.4 0.0 copy-start.5
  2.4 0.0 copy-start.8
  2.4 0.0 copy-start.10
  2.4 3.5 %fusion.21 = bf16[4,112,128]{2,1,0:T(8,128)(2,1)S(1)} fusion(bf16[4,4096,128]{2,0,1:T(4,128)(2,1)} %bitcast.64, f32[4096]{0:T(1024)} %param.17, f32[112]{0:T(128)S(1)} %add_rsqrt_fusion, bf16[1,4096]{1,0:T(2,128)(2,1)} %param.16, bf16[96,4096]{1,0:T(8,128)(2,1)} %param.15, bf16[112]{0:T(256)(128)(2,1)S(1)} %pad.6.clone), kind=kOutput, calls=%fused_computation.16 | convolution fusion | flops 473948160 | bytes 5120672 | tf_op jit(solution)/shard_map/nd,gdk->gnk/dot_general | solution.py:27
  5.9 0.0 copy-start.6
  5.9 0.0 copy-done.4
  6.0 0.0 copy-done.5
  6.0 0.4 copy-done.8
  6.4 0.0 copy-done.10
  6.4 0.0 copy-start.9
  6.4 0.9 fusion.24
  7.3 0.0 copy-done.6
  7.3 0.0 copy-start.7
  7.3 0.7 copy.101
  7.9 22.5 %gather_rows.1.q_ref = bf16[8,112,512]{2,1,0:T(8,128)(2,1)} custom-call(bf16[112,512]{1,0:T(8,128)(2,1)} %bitcast.52), custom_call_target="tpu_custom_call" | custom-call | tf_op jit(solution)/shard_map/gather_rows/pallas_call | solution.py:128
  30.4 0.9 slice.25
  31.3 0.0 copy-done.9
  31.3 0.6 fusion.28
  31.9 0.0 copy-done.7
  32.0 0.1 broadcast_compare_fusion
  32.0 0.1 multiply_reduce_fusion
  32.2 0.1 fusion.38
  32.3 3.1 %fusion.18 = bf16[2,112,256]{2,1,0:T(8,128)(2,1)S(1)} fusion(bf16[2,4096,256]{2,0,1:T(2,128)(2,1)} %bitcast.66, f32[4096]{0:T(1024)S(1)} %copy-done.10, f32[112]{0:T(128)S(1)} %add_rsqrt_fusion, bf16[1,4096]{1,0:T(2,128)(2,1)S(1)} %copy-done.5, bf16[96,4096]{1,0:T(8,128)(2,1)S(1)} %copy-done.4, bf16[112]{0:T(256)(128)(2,1)S(1)} %pad.6.clone), kind=kOutput, calls=%fused_computation.15 | convolution fusion | flops 473948160 | bytes 5120672 | tf_op jit(solution)/shard_map/nd,gdk->gnk/dot_general | solution.py:27
  35.4 0.0 copy-start.1
  35.4 0.6 constant_dynamic-update-slice_fusion
  36.0 0.0 copy-done
  36.0 0.3 fusion.27
  36.3 0.2 fusion.33
  36.5 0.1 fusion.37
  36.6 0.1 copy.57
  36.7 0.1 copy.59
  36.8 0.1 copy.56
  36.9 0.1 copy.58
  37.0 0.1 pad.3.clone
  37.1 0.7 maximum_maximum_fusion.1.step
  37.8 0.7 slice_bitcast_fusion
  38.4 0.6 slice.30.fk_ref
  39.7 0.6 compare_select_fusion.bias_ref
  40.3 0.5 iota_add_fusion.1.own_ref
  40.8 0.0 copy-done.1
  40.8 0.0 copy-start.2
  40.9 1.6 %copy.100 = bf16[2048,2,256]{2,0,1:T(8,128)(2,1)} copy(bf16[2048,2,256]{2,1,0:T(2,128)(2,1)S(1)} %copy-done.1) | data formatting | bytes 4194304 | tf_op args[10]
  42.4 0.8 copy-done.2
  43.2 1.6 %copy.50 = bf16[2,2,2048,128]{3,2,1,0:T(8,128)(2,1)} copy(bf16[2,2,2048,128]{3,1,0,2:T(2,128)(2,1)S(1)} %bitcast.50) | data formatting | bytes 4194304 | tf_op jit(solution)/shard_map/transpose | solution.py:564
  44.8 18.1 %attend.1 = (bf16[8,96,1024]{2,1,0:T(8,128)(2,1)}, f32[2,8,384]{2,1,0:T(8,128)}) custom-call(bf16[8,112,512]{2,1,0:T(8,128)(2,1)} %gather_rows.1.q_ref, bf16[4,2048,128]{2,1,0:T(8,128)(2,1)} %bitcast.48, bf16[2,2048,256]{2,1,0:T(8,128)(2,1)} %bitcast.47, bf16[4,96,128]{2,1,0:T(8,128)(2,1)} %slice.30.fk_ref, bf16[2,96,256]{2,1,0:T(8,128)(2,1)} %get-tuple-element.33.fv_ref, ...), custom_call_target="tpu_custom_call" | custom-call | tf_op jit(solution)/shard_map/attend/pallas_call | solution.py:188
  62.9 31.2 %exchange.1.heads = bf16[112,512]{1,0:T(8,128)(2,1)} custom-call(f32[1,2]{1,0:T(1,128)} %bitcast.63, f32[1,256]{1,0:T(1,128)} %bitcast.62, bf16[8,96,1024]{2,1,0:T(8,128)(2,1)} %get-tuple-element.8.vals, f32[2,8,384]{2,1,0:T(8,128)} %get-tuple-element.9.stats, f32[8,4,384]{2,1,0:T(4,128)} %maximum_maximum_fusion.1.step), custom_call_target="tpu_custom_call" | custom-call | tf_op jit(solution)/shard_map/exchange/pallas_call | solution.py:415
  94.1 0.0 copy-start.3
  94.1 13.2 %project_out.1 = bf16[112,1024]{1,0:T(8,128)(2,1)} custom-call(bf16[112,512]{1,0:T(8,128)(2,1)} %exchange.1.heads, bf16[512,4096]{1,0:T(8,128)(2,1)} %bitcast.49), custom_call_target="tpu_custom_call" | custom-call | tf_op jit(solution)/shard_map/project_out/pallas_call | solution.py:496
  107.3 1.6 %slice.28 = bf16[96,1024]{1,0:T(8,128)(2,1)} slice(bf16[112,1024]{1,0:T(8,128)(2,1)} %project_out.1), slice={[0:96], [0:1024]} | slice | bytes 393216 | tf_op jit(solution)/shard_map/slice | solution.py:637
  108.9 1.3 %slice.29 = bf16[1,1024]{1,0:T(2,128)(2,1)} slice(bf16[112,1024]{1,0:T(8,128)(2,1)} %project_out.1), slice={[96:97], [0:1024]} | slice | bytes 4096 | tf_op jit(solution)/shard_map/slice | solution.py:637
  110.2 0.7 copy.61
  111.0 0.0 copy-done.3
  111.0 0.7 copy.60
  (16 shorter events, 0.1 us)
Async XLA Ops:
  0.6 35.3 %copy-start = (bf16[8,128,2,256]{3,2,1,0:T(2,128)(2,1)S(1)}, bf16[8,128,2,256]{3,2,1,0:T(2,128)(2,1)}, u32[]{:S(2)}) copy-start(bf16[8,128,2,256]{3,2,1,0:T(2,128)(2,1)} %param.27) | copy-start | bytes 3145732
  2.4 3.6 %copy-start.4 = (bf16[96,4096]{1,0:T(8,128)(2,1)S(1)}, bf16[96,4096]{1,0:T(8,128)(2,1)}, u32[]{:S(2)}) copy-start(bf16[96,4096]{1,0:T(8,128)(2,1)} %param.15) | copy-start | bytes 2359300
  2.4 3.6 %copy-start.5 = (bf16[1,4096]{1,0:T(2,128)(2,1)S(1)}, bf16[1,4096]{1,0:T(2,128)(2,1)}, u32[]{:S(2)}) copy-start(bf16[1,4096]{1,0:T(2,128)(2,1)} %param.16) | copy-start | bytes 24580
  2.4 4.0 %copy-start.8 = (bf16[4096,2,2,128]{3,2,1,0:T(2,128)(2,1)S(1)}, bf16[4096,2,2,128]{3,2,1,0:T(2,128)(2,1)}, u32[]{:S(2)}) copy-start(bf16[4096,2,2,128]{3,2,1,0:T(2,128)(2,1)} %param.18) | copy-start | bytes 12582916
  2.4 4.0 %copy-start.10 = (f32[4096]{0:T(1024)S(1)}, f32[4096]{0:T(1024)}, u32[]{:S(2)}) copy-start(f32[4096]{0:T(1024)} %param.17) | copy-start | bytes 49156
  5.9 1.4 %copy-start.6 = (bf16[4,1,128]{2,0,1:T(4,128)(2,1)}, bf16[4,1,128]{2,0,1:T(4,128)(2,1)S(1)}, u32[]{:S(2)}) copy-start(bf16[4,1,128]{2,0,1:T(4,128)(2,1)S(1)} %copy.68) | copy-start | bytes 3076
  6.4 24.9 %copy-start.9 = (bf16[8,128,2,2,128]{4,3,2,1,0:T(2,128)(2,1)S(1)}, bf16[8,128,2,2,128]{4,3,2,1,0:T(2,128)(2,1)}, u32[]{:S(2)}) copy-start(bf16[8,128,2,2,128]{4,3,2,1,0:T(2,128)(2,1)} %param.26) | copy-start | bytes 3145732
  7.3 24.7 %copy-start.7 = (s32[8]{0:T(128)S(1)}, s32[8]{0:T(128)}, u32[]{:S(2)}) copy-start(s32[8]{0:T(128)} %param.29) | copy-start | bytes 100
  35.4 5.5 %copy-start.1 = (bf16[2048,2,256]{2,1,0:T(2,128)(2,1)S(1)}, bf16[2048,2,256]{2,1,0:T(2,128)(2,1)}, u32[]{:S(2)}) copy-start(bf16[2048,2,256]{2,1,0:T(2,128)(2,1)} %param.25) | copy-start | bytes 6291460
  40.8 2.3 %copy-start.2 = (bf16[2048,2,2,128]{3,2,1,0:T(2,128)(2,1)S(1)}, bf16[2048,2,2,128]{3,2,1,0:T(2,128)(2,1)}, u32[]{:S(2)}) copy-start(bf16[2048,2,2,128]{3,2,1,0:T(2,128)(2,1)} %param.24) | copy-start | bytes 6291460
  94.1 16.9 %copy-start.3 = (bf16[4,96,128]{2,1,0:T(8,128)(2,1)S(1)}, bf16[4,96,128]{2,1,0:T(8,128)(2,1)}, u32[]{:S(2)}) copy-start(bf16[4,96,128]{2,1,0:T(8,128)(2,1)} %slice.30.fk_ref) | copy-start | bytes 294916
